TPU v7x, 256 devices: a whole 4x4x8 slice. The times are simulated.
256 devices in a mesh: sp: 32 (over z, x), tp: 8 (over y, core).
Axes of the slice: x: 4, y: 4, z: 8, core: 2. Of those that a mesh axis runs over, the one named last changes fastest.
Arguments:
- resid: bfloat16 [8192, 4096], P('sp'), may hold values from -6 to 6
- queries: bfloat16 [8192, 3072], P('sp', 'tp'), may hold values from -1000 to 1000
- latent: bfloat16 [8192, 512], P('sp'), may hold values from -6 to 6
- rope_key: bfloat16 [8192, 64], P('sp'), may hold values from -6 to 6
- lat_gain: float32 [512], replicated, may hold values from 0.1 to 1.9
- kv_weight: bfloat16 [512, 4096], P(None, 'tp'), may hold values from -4 to 4
- out_gain: float32 [2048], P('tp'), may hold values from 0.1 to 1.9
- out_weight: bfloat16 [2048, 4096], P('tp'), may hold values from -0.125 to 0.125
- ffn_gain: float32 [4096], replicated, may hold values from 0.1 to 1.9
- gate_weight: bfloat16 [4096, 6144], P('sp', 'tp'), may hold values from -0.09375 to 0.09375
- up_weight: bfloat16 [4096, 6144], P('sp', 'tp'), may hold values from -0.09375 to 0.09375
- down_weight: bfloat16 [6144, 4096], P('tp', 'sp'), may hold values from -0.078125 to 0.078125
Outputs:
- result: bfloat16 [8192, 4096], P(('sp', 'tp'))
All inputs are finite; a program needn't handle non-finite values.
Results may differ from a plain program's by a relative error of at most 0.018.
Values may be sent and summed in bfloat16 or wider, within the bound.
A program may use at most 192 MiB of HBM per device.

v0:
```python
import math

import jax
import jax.numpy as jnp
from jax import lax
from jax.sharding import PartitionSpec as P

HEADS = 16
NOPE = 128
ROPE = 64
VDIM = 128


EPSILON = 1e-06
THETA = 10000.0
LOWEST = -1e30


def turned_gather(arrays, axis, dims):
    turned = [jnp.moveaxis(a, dim, 0) for a, dim in zip(arrays, dims)]
    both = jnp.concatenate([t.reshape(len(t), -1) for t in turned], axis=1)
    filled, at, outs = (lax.all_gather(both, axis, axis=0, tiled=True), 0, [])
    for t, dim in zip(turned, dims):
        slab = filled[:, at : at + t[0].size].reshape(-1, *t.shape[1:])
        outs.append(jnp.moveaxis(slab, 0, dim))
        at += t[0].size
    return tuple(outs)


def side_by_side(arrays, axis, dim, along):
    ends, at = ([], 0)
    for a in arrays[:-1]:
        at += a.shape[along]
        ends.append(at)
    both = jnp.concatenate(arrays, axis=along)
    return tuple(jnp.split(lax.all_gather(both, axis, axis=dim, tiled=True), ends, axis=along))


def sent_to_all(array, axis):
    copies = jnp.broadcast_to(array, (lax.axis_size(axis), *array.shape))
    return lax.all_to_all(copies, axis, split_axis=0, concat_axis=0, tiled=True)


def over_copies(array, axis):
    return sent_to_all(array, axis).sum(axis=0)


def cut_along(array, dim, devices):
    shape = array.shape
    parts = array.reshape(*shape[:dim], devices, shape[dim] // devices, *shape[dim + 1 :])
    return jnp.moveaxis(parts, dim, 0)


def summed_on_arrival(array, axis, dim):
    parts = cut_along(array, dim, lax.axis_size(axis))
    arrived = lax.all_to_all(parts, axis, split_axis=0, concat_axis=0, tiled=True)
    return arrived.astype(jnp.float32).sum(axis=0)


def laid_out(parts, dim):
    shape = list(parts.shape[1:])
    shape[dim] *= parts.shape[0]
    return jnp.moveaxis(parts, 0, dim).reshape(shape)


def gather_directly(array, axis, dim):
    parts = sent_to_all(array, axis)
    return laid_out(parts, dim)


def rotate(values, places):
    half = values.shape[-1] // 2
    inverse = THETA ** (-jnp.arange(half, dtype=jnp.float32) / half)
    angle = places[..., None] * inverse
    cosine = jnp.cos(angle)
    sine = jnp.sin(angle)
    first = values[..., :half]
    second = values[..., half:]
    return jnp.concatenate(
        [first * cosine - second * sine, first * sine + second * cosine], axis=-1
    )


def norm_rows(values, gain):
    wide = values.astype(jnp.float32)
    return wide * lax.rsqrt(jnp.mean(wide * wide, axis=-1, keepdims=True) + EPSILON) * gain


def make_keys(latent_piece, rotary_piece, start, lat_gain, kv_weight):
    normed = norm_rows(latent_piece, lat_gain).astype(jnp.bfloat16)
    key_value = jnp.dot(normed, kv_weight, preferred_element_type=jnp.float32).astype(jnp.bfloat16)
    key_index = start + jnp.arange(latent_piece.shape[0], dtype=jnp.int32)
    key_rope = rotate(rotary_piece.astype(jnp.float32), key_index.astype(jnp.float32)).astype(
        jnp.bfloat16
    )
    return (key_value, key_rope)


def body(
    resid,
    queries,
    latent,
    rope_key,
    lat_gain,
    kv_weight,
    out_gain,
    out_weight,
    ffn_gain,
    gate_weight,
    up_weight,
    down_weight,
):
    rows_here = resid.shape[0]
    first_row = lax.axis_index("sp") * rows_here
    heads_here = queries.shape[1] // (NOPE + ROPE)
    whole_gate, whole_up, whole_down = turned_gather(
        (gate_weight, up_weight, down_weight), "sp", (0, 0, 1)
    )
    query = queries.reshape(rows_here, heads_here, NOPE + ROPE)
    query_index = first_row + jnp.arange(rows_here, dtype=jnp.int32)
    query_nope = query[:, :, :NOPE]
    query_rope = rotate(
        query[:, :, NOPE:].astype(jnp.float32), query_index.astype(jnp.float32)[:, None]
    ).astype(jnp.bfloat16)
    scale = 1.0 / math.sqrt(NOPE + ROPE)

    def accumulate(state, key_value, key_rope):
        running_max, running_sum, weighted = state
        length = key_value.shape[0]
        key_value = key_value.reshape(length, heads_here, NOPE + VDIM)
        key_index = jnp.arange(length, dtype=jnp.int32)
        scores = jnp.einsum(
            "qhd,khd->hqk", query_nope, key_value[:, :, :NOPE], preferred_element_type=jnp.float32
        )
        scores = (
            scores
            + jnp.einsum("qhr,kr->hqk", query_rope, key_rope, preferred_element_type=jnp.float32)
        ) * scale
        allowed = (key_index[None, :] <= query_index[:, None])[None]
        scores = jnp.where(allowed, scores, LOWEST)
        new_max = jnp.maximum(running_max, jnp.max(scores, axis=-1))
        weights = jnp.where(allowed, jnp.exp(scores - new_max[:, :, None]), 0.0)
        running_sum = jnp.sum(weights, axis=-1)
        added = jnp.einsum(
            "hqk,khd->qhd",
            weights.astype(jnp.bfloat16),
            key_value[:, :, NOPE:],
            preferred_element_type=jnp.float32,
        )
        weighted = added
        return (new_max, running_sum, weighted)

    def unchanged(state):
        return state

    initial = (
        jnp.full((heads_here, rows_here), LOWEST, jnp.float32),
        jnp.zeros((heads_here, rows_here), jnp.float32),
        jnp.zeros((rows_here, heads_here, VDIM), jnp.float32),
    )
    own_value, own_rope = make_keys(latent, rope_key, first_row, lat_gain, kv_weight)
    pieces = side_by_side((own_value, own_rope), "sp", 0, 1)

    def update(state):
        return accumulate(state, pieces[0], pieces[1])

    running_max, running_sum, weighted = lax.cond(
        jnp.int32(0) < first_row + rows_here, update, unchanged, initial
    )
    attended = (weighted / jnp.transpose(running_sum)[:, :, None]).astype(jnp.bfloat16)
    attended_float = attended.reshape(rows_here, heads_here * VDIM).astype(jnp.float32)
    squares = over_copies(jnp.sum(attended_float * attended_float, axis=1), "tp")
    normed_out = attended_float * lax.rsqrt(squares / (HEADS * VDIM) + EPSILON)[:, None] * out_gain
    normed_out = normed_out.astype(jnp.bfloat16)
    share = rows_here // lax.axis_size("tp")
    own_first = lax.axis_index("tp") * share
    attn_sum = summed_on_arrival(
        jnp.dot(normed_out, out_weight, preferred_element_type=jnp.float32).astype(jnp.bfloat16),
        "tp",
        0,
    )
    own_resid = lax.dynamic_slice_in_dim(resid, own_first, share, 0)
    middle = (own_resid.astype(jnp.float32) + attn_sum).astype(jnp.bfloat16)
    normed_mid = gather_directly(norm_rows(middle, ffn_gain).astype(jnp.bfloat16), "tp", 0)
    gate = jnp.dot(normed_mid, whole_gate, preferred_element_type=jnp.float32)
    upward = jnp.dot(normed_mid, whole_up, preferred_element_type=jnp.float32)
    hidden = (jax.nn.silu(gate) * upward).astype(jnp.bfloat16)
    terms = jnp.dot(hidden, whole_down, preferred_element_type=jnp.float32)
    ffn_sum = summed_on_arrival(terms.astype(jnp.bfloat16), "tp", 0)
    return (middle.astype(jnp.float32) + ffn_sum).astype(jnp.bfloat16)


def solution(mesh):
    placed = (
        P("sp", None),
        P("sp", "tp"),
        P("sp", None),
        P("sp", None),
        P(),
        P(None, "tp"),
        P("tp"),
        P("tp", None),
        P(),
        P("sp", "tp"),
        P("sp", "tp"),
        P("tp", "sp"),
    )
    return jax.shard_map(
        body, mesh=mesh, in_specs=placed, out_specs=P(("sp", "tp"), None), check_vma=False
    )
```

profile of v0, /device:TPU:1, one launch (start us, length us, event | category | flops | bytes accessed | tf_op | source)
XLA Modules:
  0.0 339.7 jit_solution(4206966190794154403)
XLA Ops:
  6.5 0.0 copy-start
  6.5 0.0 all-gather.3.cloned.1.call-start
  6.6 0.9 convert_element_type.86
  7.5 0.2 multiply_cosine_fusion
  7.7 0.1 copy.62
  7.8 0.1 copy.63
  7.9 1.1 fusion.41
  9.0 1.5 convolution_convert_fusion.1
  10.5 0.8 pad_maximum_fusion.1
  11.4 0.0 all-gather.3.cloned.1.call-update
  11.4 0.0 all-gather.5.cloned.1.call-start
  11.4 1.1 copy.68
  12.5 1.1 copy.69
  13.6 1.8 pad_maximum_fusion
  15.4 0.0 all-gather.5.cloned.1.call-update
  15.4 1.1 copy.61
  16.6 106.4 %all-gather.3.cloned.1.call-done = bf16[8192,576]{1,0:T(8,128)(2,1)} async-done(((bf16[256,576]{1,0:T(8,128)(2,1)}), bf16[8192,576]{1,0:T(8,128)(2,1)}) %all-gather.3.cloned.1.call-update) | async-done | bytes 9437200 | tf_op jit(solution)/shard_map/all_gather | solution.py:36
  123.0 0.0 copy-start.3
  123.0 65.7 %conditional.1 = (f32[2,256]{1,0:T(2,128)S(1)}, f32[256,2,128]{0,2,1:T(8,128)S(1)}) conditional(s32[]{:T(128)} %convert_element_type.82, () %tuple.13, (s32[]{:T(128)}, s32[256]{0:T(256)S(1)}, bf16[256,2,192]{0,2,1:T(8,128)(2,1)S(1)}, bf16[8192,576]{1,0:T(8,128)(2,1)}, bf16[256,2,64]{0,2,1:T(8,128)(2,1)S(1)}) %tuple.36), branch_computations={%region_1.0_spmd, %region_2.5_spmd} | conditional | flops 2728394496 | bytes 147143728 | solution.py:167
  123.0 13.1 %copy.65 = bf16[8192,576]{0,1:T(8,128)(2,1)} copy(bf16[8192,576]{1,0:T(8,128)(2,1)} %get-tuple-element.53) | data formatting | bytes 18874368 | tf_op jit(solution)/shard_map
  136.1 7.9 %split.8 = bf16[8192,512]{0,1:T(8,128)(2,1)} slice(bf16[8192,576]{0,1:T(8,128)(2,1)} %copy.65), slice={[0:8192], [0:512]} | slice | bytes 16777216 | tf_op jit(solution)/shard_map/split | solution.py:36
  144.0 2.6 iota_compare_fusion
  146.6 9.4 %fusion.16 = f32[8192,256,2]{0,1,2:T(8,128)} fusion(bf16[256,2,64]{0,2,1:T(8,128)(2,1)S(1)} %get-tuple-element.25, bf16[8192,576]{0,1:T(8,128)(2,1)} %copy.65), kind=kOutput, calls=%fused_computation.15 | convolution fusion | flops 536870912 | bytes 17891328 | tf_op jit(solution)/shard_map/cond/branch_1_fun/qhr,kr->hqk/dot_general | solution.py:137
  156.0 0.1 copy.64
  156.2 0.0 copy-start.1
  156.2 15.2 %fusion.57 = (f32[2,256]{1,0:T(2,128)S(1)}, f32[2,256,8192]{2,1,0:T(8,128)}) fusion(f32[8192,256,2]{0,1,2:T(8,128)} %fusion.16, bf16[8192,2,256]{0,2,1:T(8,128)(2,1)} %bitcast.30, bf16[256,2,192]{2,0,1:T(8,128)(2,1)S(1)} %copy.64, pred[256,8192]{1,0:T(8,128)(4,1)} %iota_compare_fusion), kind=kOutput, calls=%fused_computation.76 | convolution fusion | flops 1090518528 | bytes 39979008 | tf_op jit(solution)/shard_map/cond/branch_1_fun/qhd,khd->hqk/dot_general | solution.py:132
  171.3 0.0 copy-done.1
  171.3 8.6 %fusion.11 = f32[256,2,128]{2,0,1:T(8,128)S(1)} fusion(bf16[8192,2,256]{0,2,1:T(8,128)(2,1)} %bitcast.31, f32[2,256,8192]{2,1,0:T(8,128)} %get-tuple-element.61, f32[2,256]{1,0:T(2,128)S(1)} %broadcast_maximum_fusion, pred[256,8192]{1,0:T(8,128)(4,1)S(1)} %copy-done.1), kind=kOutput, calls=%fused_computation.13 | convolution fusion | flops 1086324736 | bytes 23332864 | tf_op jit(solution)/shard_map/cond/branch_1_fun/hqk,khd->qhd/dot_general | solution.py:144
  180.0 0.1 copy.72
  180.1 8.5 %fusion.3 = f32[2,256]{1,0:T(2,128)S(1)} fusion(f32[2,256,8192]{2,1,0:T(8,128)} %get-tuple-element.61, f32[2,256]{1,0:T(2,128)S(1)} %broadcast_maximum_fusion, pred[256,8192]{1,0:T(8,128)(4,1)} %iota_compare_fusion), kind=kLoop, calls=%fused_computation.5 | loop fusion | flops 12582400 | bytes 18878464 | tf_op jit(solution)/shard_map/cond/branch_1_fun/reduce_sum | solution.py:143
  188.6 0.1 multiply_reduce_fusion
  188.7 10.3 %all_to_all.21 = f32[8,1,256]{2,1,0:T(1,128)S(1)} all-to-all(f32[8,1,256]{2,1,0:T(1,128)S(1)} %broadcast_in_dim.47), channel_id=1, replica_groups=mesh['sp'=32,'tp'=8] {'tp'}, dimensions={0} | all-to-all | bytes 16384 | tf_op jit(solution)/shard_map/all_to_all | solution.py:41
  199.1 0.0 copy-done.3
  199.1 0.0 copy-start.2
  199.1 0.1 fusion.51
  199.2 0.0 copy-done
  199.2 2.1 convolution_convert_fusion
  201.3 4.9 %all-to-all-start.1 = ((bf16[8,32,4096]{2,1,0:T(8,128)(2,1)}), bf16[8,32,4096]{2,1,0:T(8,128)(2,1)}, u32[]{:S(2)}, u32[]{:S(2)}) async-start(bf16[8,32,4096]{2,1,0:T(8,128)(2,1)} %bitcast.32), calls=%async_computation.1 | async-start | bytes 4194304 | tf_op jit(solution)/shard_map/all_to_all | solution.py:56
  206.1 26.3 %all-to-all-done.1 = bf16[8,32,4096]{2,1,0:T(8,128)(2,1)} async-done(((bf16[8,32,4096]{2,1,0:T(8,128)(2,1)}), bf16[8,32,4096]{2,1,0:T(8,128)(2,1)}, u32[]{:S(2)}, u32[]{:S(2)}) %all-to-all-start.1) | async-done | bytes 2097184 | tf_op jit(solution)/shard_map/all_to_all | solution.py:56
  232.5 2.0 convert_reduce_fusion.1
  234.5 1.2 fusion.44
  235.6 0.0 copy-done.2
  235.6 0.1 fusion.46
  235.8 0.2 broadcast_in_dim.48
  236.0 30.3 %all_to_all.22 = bf16[8,32,4096]{2,1,0:T(8,128)(2,1)} all-to-all(bf16[8,32,4096]{2,1,0:T(8,128)(2,1)S(1)} %broadcast_in_dim.48), channel_id=1, replica_groups=mesh['sp'=32,'tp'=8] {'tp'}, dimensions={0} | all-to-all | bytes 4194304 | tf_op jit(solution)/shard_map/all_to_all | solution.py:41
  266.3 14.7 %all-gather.5.cloned.1.call-done = bf16[4096,2304]{0,1:T(8,128)(2,1)} async-done(((bf16[128,2304]{0,1:T(8,128)(2,1)}), bf16[4096,2304]{0,1:T(8,128)(2,1)}) %all-gather.5.cloned.1.call-update) | async-done | bytes 18874384 | tf_op jit(solution)/shard_map/all_gather | solution.py:22
  281.0 5.2 %fusion.23 = f32[256,768]{1,0:T(8,128)S(1)} fusion(bf16[256,4096]{1,0:T(8,128)(2,1)} %bitcast.33, bf16[4096,2304]{0,1:T(8,128)(2,1)} %all-gather.5.cloned.1.call-done), kind=kOutput, calls=%fused_computation.24 | convolution fusion | flops 1610612736 | bytes 9175040 | tf_op jit(solution)/shard_map/dot_general | solution.py:185
  286.2 11.1 %fusion.25 = bf16[256,4096]{1,0:T(8,128)(2,1)} fusion(bf16[4096,2304]{0,1:T(8,128)(2,1)} %all-gather.5.cloned.1.call-done, bf16[256,4096]{1,0:T(8,128)(2,1)} %bitcast.34, f32[256,768]{1,0:T(8,128)S(1)} %fusion.23), kind=kOutput, calls=%fused_computation.27 | convolution fusion | flops 3223453696 | bytes 17563648 | tf_op jit(solution)/shard_map/dot_general | solution.py:188
  297.3 34.5 %all_to_all.23 = bf16[8,32,4096]{2,1,0:T(8,128)(2,1)S(1)} all-to-all(bf16[8,32,4096]{2,1,0:T(8,128)(2,1)} %bitcast.35), channel_id=1, replica_groups=mesh['sp'=32,'tp'=8] {'tp'}, dimensions={0} | all-to-all | bytes 4194304 | tf_op jit(solution)/shard_map/all_to_all | solution.py:56
  331.8 0.3 convert_reduce_fusion
  332.1 0.8 fusion.47
  (13 shorter events, 0.1 us)
Async XLA Ops:
  6.5 192.7 %copy-start = (bf16[256,4096]{1,0:T(8,128)(2,1)S(1)}, bf16[256,4096]{1,0:T(8,128)(2,1)}, u32[]{:S(2)}) copy-start(bf16[256,4096]{1,0:T(8,128)(2,1)} %param.21) | copy-start | bytes 6291460
  6.5 116.4 %all-gather.3.cloned.1.call-start = ((), (), s32[]{:S(2)}) async-start(), calls=%async_computation.4 | async-start | bytes 10813440 | tf_op jit(solution)/shard_map/all_gather | solution.py:36
  11.4 269.6 %all-gather.5.cloned.1.call-start = ((), (), s32[]{:S(2)}) async-start(), calls=%async_computation.5 | async-start | bytes 19464192 | tf_op jit(solution)/shard_map/all_gather | solution.py:22
  123.0 76.1 %copy-start.3 = (f32[256]{0:T(256)S(1)}, f32[256]{0:T(256)}, u32[]{:S(2)}) copy-start(f32[256]{0:T(256)} %param.20) | copy-start | bytes 3076
  156.2 15.2 %copy-start.1 = (pred[256,8192]{1,0:T(8,128)(4,1)S(1)}, pred[256,8192]{1,0:T(8,128)(4,1)}, u32[]{:S(2)}) copy-start(pred[256,8192]{1,0:T(8,128)(4,1)} %iota_compare_fusion) | copy-start | bytes 6291460 | tf_op jit(solution)/shard_map/cond
  199.1 36.5 %copy-start.2 = (f32[4096]{0:T(1024)S(1)}, f32[4096]{0:T(1024)}, u32[]{:S(2)}) copy-start(f32[4096]{0:T(1024)} %param.22) | copy-start | bytes 49156
  201.3 31.2 %all-to-all-start.1 = ((bf16[8,32,4096]{2,1,0:T(8,128)(2,1)}), bf16[8,32,4096]{2,1,0:T(8,128)(2,1)}, u32[]{:S(2)}, u32[]{:S(2)}) async-start(bf16[8,32,4096]{2,1,0:T(8,128)(2,1)} %bitcast.32), calls=%async_computation.1 | async-start | bytes 4194304 | tf_op jit(solution)/shard_map/all_to_all | solution.py:56
Sparse Core Ops, SparseCore 0:
  11.5 111.4 all-gather.2
  125.4 155.4 all-gather.4
where the time goes:
time: 341 us; the launch traced here: 340 us
  waiting for transfers between devices  147 us (43%)
  blocking collectives  75.1 us (22%)
  matrix products  53.1 us (16%)
  local copies, waits for them, and re-layouts  25 us (7%)
  other arithmetic  20.6 us (6%)
  between operations  13.5 us (4%)
  starting transfers between devices  4.9 us (1%)
    all_gather x1, waiting for transfers between devices, side_by_side(): lax.all_gather(both, axis, axis=dim, tiled=True)  106 us
    all_to_all x2, blocking collectives, sent_to_all(): return lax.all_to_all(copies, axis, split_axis=0, concat_axis=0, tiled=True)  40.6 us
    all_to_all x1, blocking collectives, summed_on_arrival(): lax.all_to_all(parts, axis, split_axis=0, concat_axis=0, tiled=True)  34.5 us
    all_to_all x1, waiting for transfers between devices, summed_on_arrival(): lax.all_to_all(parts, axis, split_axis=0, concat_axis=0, tiled=True)  26.3 us
    dot_general x1, matrix products, accumulate(): jnp.einsum('qhd,khd->hqk', query_nope, key_value[:, :, :NOPE], preferred_...  15.2 us
    all_gather x1, waiting for transfers between devices, turned_gather(): filled, at, outs = (lax.all_gather(both, axis, axis=0, tiled=True), 0, [])  14.7 us
    another operation x4, local copies, waits for them, and re-layouts  13.5 us
    dot_general x1, matrix products, body(): terms = jnp.dot(hidden, whole_down, preferred_element_type=jnp.float32)  11.1 us
  transfers between devices with their start and end apart: 3, of which 3 were waited for; matrix products, arithmetic and copies ran while one was open for 23% of the time, Pallas kernels for 0%

commit v1 on v0

v1 whole, which is shorter than its diff:
```python
import functools
import math

import jax
import jax.numpy as jnp
from jax import lax
from jax.experimental import pallas as pl
from jax.experimental.pallas import tpu as pltpu
from jax.sharding import PartitionSpec as P

HEADS = 16
NOPE = 128
ROPE = 64
VDIM = 128
NX = 4
NC = 2
CHUNKS = 2

EPSILON = 1e-06
THETA = 10000.0
LOWEST = -1e30
MESH = pl.DeviceIdType.MESH
F32 = jnp.float32
BF16 = jnp.bfloat16


def turned_gather(arrays, axis, dims):
    turned = [jnp.moveaxis(a, dim, 0) for a, dim in zip(arrays, dims)]
    both = jnp.concatenate([t.reshape(len(t), -1) for t in turned], axis=1)
    filled, at, outs = (lax.all_gather(both, axis, axis=0, tiled=True), 0, [])
    for t, dim in zip(turned, dims):
        slab = filled[:, at : at + t[0].size].reshape(-1, *t.shape[1:])
        outs.append(jnp.moveaxis(slab, 0, dim))
        at += t[0].size
    return tuple(outs)


def sent_to_all(array, axis):
    copies = jnp.broadcast_to(array, (lax.axis_size(axis), *array.shape))
    return lax.all_to_all(copies, axis, split_axis=0, concat_axis=0, tiled=True)


def over_copies(array, axis):
    return sent_to_all(array, axis).sum(axis=0)


def cut_along(array, dim, devices):
    shape = array.shape
    parts = array.reshape(*shape[:dim], devices, shape[dim] // devices, *shape[dim + 1 :])
    return jnp.moveaxis(parts, dim, 0)


def summed_on_arrival(array, axis, dim):
    parts = cut_along(array, dim, lax.axis_size(axis))
    arrived = lax.all_to_all(parts, axis, split_axis=0, concat_axis=0, tiled=True)
    return arrived.astype(jnp.float32).sum(axis=0)


def laid_out(parts, dim):
    shape = list(parts.shape[1:])
    shape[dim] *= parts.shape[0]
    return jnp.moveaxis(parts, 0, dim).reshape(shape)


def gather_directly(array, axis, dim):
    parts = sent_to_all(array, axis)
    return laid_out(parts, dim)


def norm_rows(values, gain):
    wide = values.astype(jnp.float32)
    return wide * lax.rsqrt(jnp.mean(wide * wide, axis=-1, keepdims=True) + EPSILON) * gain


def nt_dot(a, b):
    return lax.dot_general(a, b, (((1,), (1,)), ((), ())), preferred_element_type=F32)


def attention_kernel(
    nz,
    lat_ref,
    q_ref,
    wk_ref,
    wv_ref,
    out_ref,
    latbuf,
    qbuf,
    acc,
    stat_m,
    stat_l,
    osend,
    orecv,
    ssend,
    srecv,
    local_sem,
    ring_send,
    ring_recv,
    pair_send,
    pair_recv,
    q_send,
    q_recv,
    o_send,
    o_recv,
    s_send,
    s_recv,
):
    sp = lax.axis_index("sp")
    tp = lax.axis_index("tp")
    z, x = sp // NX, lax.rem(sp, NX)
    core = lax.rem(tp, NC)
    up = lax.rem(z + 1, nz) * NX + x
    down = lax.rem(z + nz - 1, nz) * NX + x
    partner = tp + 1 - 2 * core
    rows = q_ref.shape[1]
    far = nz // 2
    factor = (1.0 / math.sqrt(NOPE + ROPE)) * math.log2(math.e)

    barrier = pltpu.get_barrier_semaphore()
    peers = [(up, tp), (down, tp), (sp, partner)]
    for k in range(1, NX):
        peers.append((z * NX + lax.rem(x + k, NX), tp))
    for peer in peers:
        pl.semaphore_signal(barrier, inc=1, device_id=peer, device_id_type=MESH)
    pl.semaphore_wait(barrier, len(peers))

    def ring(src_slot, dst_slot, chunk, device):
        src = lat_ref.at[core, chunk] if src_slot is None else latbuf.at[src_slot, core, chunk]
        return pltpu.make_async_remote_copy(
            src_ref=src,
            dst_ref=latbuf.at[dst_slot, core, chunk],
            send_sem=ring_send.at[dst_slot, chunk],
            recv_sem=ring_recv.at[dst_slot, chunk],
            device_id=(device, tp),
            device_id_type=MESH,
        )

    def pair(slot, chunk):
        return pltpu.make_async_remote_copy(
            src_ref=latbuf.at[slot, core, chunk],
            dst_ref=latbuf.at[slot, core, chunk],
            send_sem=pair_send.at[slot, chunk],
            recv_sem=pair_recv.at[slot, chunk],
            device_id=(sp, partner),
            device_id_type=MESH,
        )

    def pair_in(slot, chunk):
        return pltpu.make_async_remote_copy(
            src_ref=latbuf.at[slot, 1 - core, chunk],
            dst_ref=latbuf.at[slot, 1 - core, chunk],
            send_sem=pair_send.at[slot, chunk],
            recv_sem=pair_recv.at[slot, chunk],
            device_id=(sp, partner),
            device_id_type=MESH,
        )

    def q_copy(k):
        return pltpu.make_async_remote_copy(
            src_ref=q_ref,
            dst_ref=qbuf.at[x],
            send_sem=q_send.at[k],
            recv_sem=q_recv.at[k],
            device_id=(z * NX + lax.rem(x + k, NX), tp),
            device_id_type=MESH,
        )

    for chunk in range(CHUNKS):
        ring(None, 1, chunk, up).start()
        ring(None, far + 1, chunk, down).start()
    own_lat = pltpu.make_async_copy(lat_ref, latbuf.at[0], local_sem.at[0])
    own_q = pltpu.make_async_copy(q_ref, qbuf.at[x], local_sem.at[1])
    own_lat.start()
    own_q.start()
    for k in range(1, NX):
        q_copy(k).start()

    stat_m[...] = jnp.full(stat_m.shape, LOWEST, F32)
    stat_l[...] = jnp.zeros(stat_l.shape, F32)
    acc[...] = jnp.zeros(acc.shape, F32)

    def piece(slot, diagonal):
        lat = latbuf[slot].reshape(rows, lat_ref.shape[-1])
        wide = wk_ref.shape[0]
        compressed, key_rot = lat[:, :wide], lat[:, wide:]
        keys = jnp.dot(compressed, wk_ref[...], preferred_element_type=F32).astype(BF16)
        values = nt_dot(wv_ref[...], compressed).astype(BF16)
        for h in range(2):
            key = jnp.concatenate([keys[:, h * NOPE : (h + 1) * NOPE], key_rot], axis=1)
            value = values[h * VDIM : (h + 1) * VDIM]
            for b in range(NX):
                at = pl.ds(b * rows, rows)
                scores = nt_dot(key, qbuf[b, h]) * factor
                if diagonal:
                    key_at = x * rows + lax.broadcasted_iota(jnp.int32, scores.shape, 0)
                    query_at = b * rows + lax.broadcasted_iota(jnp.int32, scores.shape, 1)
                    allowed = key_at <= query_at
                    scores = jnp.where(allowed, scores, LOWEST)
                old = stat_m[h, :, at]
                new = jnp.maximum(old, jnp.max(scores, axis=0, keepdims=True))
                weights = jnp.exp2(scores - new)
                if diagonal:
                    weights = jnp.where(allowed, weights, 0.0)
                shrink = jnp.exp2(old - new)
                stat_m[h, :, at] = new
                stat_l[h, :, at] = stat_l[h, :, at] * shrink + jnp.sum(
                    weights, axis=0, keepdims=True
                )
                acc[h, :, at] = acc[h, :, at] * shrink + jnp.dot(
                    value, weights.astype(BF16), preferred_element_type=F32
                )

    own_lat.wait()
    own_q.wait()
    for k in range(1, NX):
        q_copy(k).wait_recv()
    piece(0, True)

    def arrive(slot, forward_to, device):
        for chunk in range(CHUNKS):
            ring(None, slot, chunk, device).wait_recv()
            if forward_to is not None:
                ring(slot, forward_to, chunk, device).start()
            pair(slot, chunk).start()

    def use(slot, needed):
        for chunk in range(CHUNKS):
            pair_in(slot, chunk).wait_recv()

        @pl.when(needed)
        def _():
            piece(slot, False)

    def both(d):
        def one(i, carry):
            slot = jnp.where(i == 0, d, far + d)
            source = jnp.where(i == 0, z - d, z + d - nz)
            use(slot, source >= 0)
            return carry

        return one

    for d in range(1, far + 1):
        arrive(d, d + 1 if d < far else None, up)
        if d < far:
            arrive(far + d, far + d + 1 if d < far - 1 else None, down)
        if d > 1:
            lax.fori_loop(0, 2, both(d - 1), 0)
    use(far, z - far >= 0)

    for k in range(1, NX):
        q_copy(k).wait_send()
    for slot in range(1, nz):
        for chunk in range(CHUNKS):
            ring(None, slot, chunk, up).wait_send()
            pair(slot, chunk).wait_send()

    for b in range(NX):
        at = pl.ds(b * rows, rows)
        for h in range(2):
            total = stat_l[h, :, at]
            inverse = jnp.where(total > 0.0, 1.0 / jnp.where(total > 0.0, total, 1.0), 0.0)
            osend[b, h * VDIM : (h + 1) * VDIM] = (acc[h, :, at] * inverse).astype(BF16)
            ssend[b, h : h + 1] = stat_m[h, :, at]
            ssend[b, 2 + h : 3 + h] = total

    def o_copy(k):
        to = lax.rem(x + k, NX)
        return pltpu.make_async_remote_copy(
            src_ref=osend.at[to],
            dst_ref=orecv.at[k],
            send_sem=o_send.at[k],
            recv_sem=o_recv.at[k],
            device_id=(z * NX + to, tp),
            device_id_type=MESH,
        )

    def s_copy(k):
        to = lax.rem(x + k, NX)
        return pltpu.make_async_remote_copy(
            src_ref=ssend.at[to],
            dst_ref=srecv.at[k],
            send_sem=s_send.at[k],
            recv_sem=s_recv.at[k],
            device_id=(z * NX + to, tp),
            device_id_type=MESH,
        )

    for k in range(1, NX):
        s_copy(k).start()
        o_copy(k).start()
    for k in range(1, NX):
        s_copy(k).wait_recv()
        o_copy(k).wait_recv()
    for h in range(2):
        stats = [ssend[x]] + [srecv[k] for k in range(1, NX)]
        outs = [osend[x, h * VDIM : (h + 1) * VDIM]] + [
            orecv[k, h * VDIM : (h + 1) * VDIM] for k in range(1, NX)
        ]
        top = functools.reduce(jnp.maximum, [s[h : h + 1] for s in stats])
        shares = [s[2 + h : 3 + h] * jnp.exp2(s[h : h + 1] - top) for s in stats]
        inverse = 1.0 / sum(shares)
        mixed = sum(o.astype(F32) * (w * inverse) for o, w in zip(outs, shares))
        out_ref[:, h * VDIM : (h + 1) * VDIM] = jnp.transpose(mixed).astype(BF16)
    for k in range(1, NX):
        s_copy(k).wait_send()
        o_copy(k).wait_send()


def attention(lat, q, wk, wv):
    nz = lax.axis_size("sp") // NX
    rows, wide = lat.shape
    lat = lat.reshape(NC, CHUNKS, rows // NC // CHUNKS, wide)
    dma = pltpu.SemaphoreType.DMA
    vmem = pl.BlockSpec(memory_space=pltpu.VMEM)
    return pl.pallas_call(
        functools.partial(attention_kernel, nz),
        out_shape=jax.ShapeDtypeStruct((rows, 2 * VDIM), BF16),
        in_specs=[vmem] * 4,
        out_specs=vmem,
        scratch_shapes=[
            pltpu.VMEM((nz, *lat.shape), BF16),
            pltpu.VMEM((NX, *q.shape), BF16),
            pltpu.VMEM((2, VDIM, NX * rows), F32),
            pltpu.VMEM((2, 1, NX * rows), F32),
            pltpu.VMEM((2, 1, NX * rows), F32),
            pltpu.VMEM((NX, 2 * VDIM, rows), BF16),
            pltpu.VMEM((NX, 2 * VDIM, rows), BF16),
            pltpu.VMEM((NX, 8, rows), F32),
            pltpu.VMEM((NX, 8, rows), F32),
            dma((2,)),
            dma((nz, CHUNKS)),
            dma((nz, CHUNKS)),
            dma((nz, CHUNKS)),
            dma((nz, CHUNKS)),
            dma((NX,)),
            dma((NX,)),
            dma((NX,)),
            dma((NX,)),
            dma((NX,)),
            dma((NX,)),
        ],
        compiler_params=pltpu.CompilerParams(
            collective_id=0, has_side_effects=True, vmem_limit_bytes=40 * 1024 * 1024
        ),
        cost_estimate=pl.CostEstimate(
            flops=20_000_000_000, bytes_accessed=4_000_000, transcendentals=0
        ),
    )(lat, q, wk, wv)


def turned(values, cosine, sine):
    half = values.shape[-1] // 2
    first, second = values[..., :half], values[..., half:]
    return jnp.concatenate(
        [first * cosine - second * sine, first * sine + second * cosine], axis=-1
    )


def attended_rows(queries, latent, rope_key, lat_gain, kv_weight):
    rows = latent.shape[0]
    first_row = lax.axis_index("sp") * rows
    heads_here = queries.shape[1] // (NOPE + ROPE)
    places = (first_row + jnp.arange(rows, dtype=jnp.int32)).astype(F32)
    half = ROPE // 2
    inverse = THETA ** (-jnp.arange(half, dtype=F32) / half)
    angle = places[:, None] * inverse
    cosine, sine = jnp.cos(angle), jnp.sin(angle)
    pad = jnp.zeros((rows, NOPE - ROPE), BF16)
    key_rot = turned(rope_key.astype(F32), cosine, sine).astype(BF16)
    normed = norm_rows(latent, lat_gain).astype(BF16)
    lat = jnp.concatenate([normed, key_rot, pad], axis=1)
    query = queries.reshape(rows, heads_here, NOPE + ROPE)
    query_rot = turned(
        query[:, :, NOPE:].astype(F32), cosine[:, None], sine[:, None]
    ).astype(BF16)
    full = jnp.concatenate(
        [query[:, :, :NOPE], query_rot, jnp.broadcast_to(pad[:, None], (rows, heads_here, NOPE - ROPE))],
        axis=2,
    )
    full = jnp.transpose(full, (1, 0, 2))
    weight = kv_weight.reshape(kv_weight.shape[0], heads_here, NOPE + VDIM)
    wk = weight[:, :, :NOPE].reshape(-1, heads_here * NOPE)
    wv = jnp.transpose(weight[:, :, NOPE:].reshape(-1, heads_here * VDIM))
    return attention(lat, full, wk, wv)


def body(
    resid,
    queries,
    latent,
    rope_key,
    lat_gain,
    kv_weight,
    out_gain,
    out_weight,
    ffn_gain,
    gate_weight,
    up_weight,
    down_weight,
):
    rows_here = resid.shape[0]
    whole_gate, whole_up, whole_down = turned_gather(
        (gate_weight, up_weight, down_weight), "sp", (0, 0, 1)
    )
    attended = attended_rows(queries, latent, rope_key, lat_gain, kv_weight)
    attended_float = attended.astype(F32)
    squares = over_copies(jnp.sum(attended_float * attended_float, axis=1), "tp")
    normed_out = attended_float * lax.rsqrt(squares / (HEADS * VDIM) + EPSILON)[:, None] * out_gain
    normed_out = normed_out.astype(jnp.bfloat16)
    share = rows_here // lax.axis_size("tp")
    own_first = lax.axis_index("tp") * share
    attn_sum = summed_on_arrival(
        jnp.dot(normed_out, out_weight, preferred_element_type=jnp.float32).astype(jnp.bfloat16),
        "tp",
        0,
    )
    own_resid = lax.dynamic_slice_in_dim(resid, own_first, share, 0)
    middle = (own_resid.astype(jnp.float32) + attn_sum).astype(jnp.bfloat16)
    normed_mid = gather_directly(norm_rows(middle, ffn_gain).astype(jnp.bfloat16), "tp", 0)
    gate = jnp.dot(normed_mid, whole_gate, preferred_element_type=jnp.float32)
    upward = jnp.dot(normed_mid, whole_up, preferred_element_type=jnp.float32)
    hidden = (jax.nn.silu(gate) * upward).astype(jnp.bfloat16)
    terms = jnp.dot(hidden, whole_down, preferred_element_type=jnp.float32)
    ffn_sum = summed_on_arrival(terms.astype(jnp.bfloat16), "tp", 0)
    return (middle.astype(jnp.float32) + ffn_sum).astype(jnp.bfloat16)


def solution(mesh):
    placed = (
        P("sp", None),
        P("sp", "tp"),
        P("sp", None),
        P("sp", None),
        P(),
        P(None, "tp"),
        P("tp"),
        P("tp", None),
        P(),
        P("sp", "tp"),
        P("sp", "tp"),
        P("tp", "sp"),
    )
    return jax.shard_map(
        body, mesh=mesh, in_specs=placed, out_specs=P(("sp", "tp"), None), check_vma=False
    )
```

time: 341 us -> 245 us (0.72)
  waiting for transfers between devices: 147 us -> 54 us
  Pallas kernels: 0 us -> 60.3 us
  matrix products: 53.1 us -> 18.4 us
  local copies, waits for them, and re-layouts: 25 us -> 10.6 us
  other arithmetic: 20.6 us -> 8.18 us
    all_gather x1 -> x0, waiting for transfers between devices: 106 us -> none  [side_by_side(): lax.all_gather(both, axis, axis=dim, tiled=True)]
    pallas_call x0 -> x1, Pallas kernels: none -> 60.3 us  [attention(): pl.pallas_call(functools.partial(attention_kernel, nz), out_shape=jax.Sha...]
    dot_general x4 -> x0, matrix products: 34.7 us -> none  [the longest x1 15.2 us: accumulate(): jnp.einsum('qhd,khd->hqk', query_nope, key_value[:, :, :NOPE], preferred_...]
    all_gather x1, waiting for transfers between devices: 14.7 us -> 27.7 us  [turned_gather(): filled, at, outs = (lax.all_gather(both, axis, axis=0, tiled=True), 0, [])]
    another operation x4 -> x2, local copies, waits for them, and re-layouts: 13.5 us -> 1.48 us
    reduce_sum x1 -> x0, other arithmetic: 8.52 us -> none  [accumulate(): running_sum = jnp.sum(weights, axis=-1)]
    split x1 -> x0, local copies, waits for them, and re-layouts: 7.9 us -> none  [side_by_side(): jnp.split(lax.all_gather(both, axis, axis=dim, tiled=True), ends, axis=al...]
  transfers between devices with their start and end apart: 3 -> 2, of which waited for: 3 -> 2; matrix products, arithmetic and copies ran while one was open for 23% -> 6% of each run, Pallas kernels for 0% -> 25%
where the time goes in v1:
time: 245 us
  blocking collectives  74.4 us (30%)
  Pallas kernels  60.3 us (25%)
  waiting for transfers between devices  54 us (22%)
  matrix products  18.4 us (8%)
  between operations  13.7 us (6%)
  local copies, waits for them, and re-layouts  10.6 us (4%)
  other arithmetic  8.18 us (3%)
  starting transfers between devices  4.96 us (2%)
    pallas_call x1, Pallas kernels, attention(): pl.pallas_call(functools.partial(attention_kernel, nz), out_shape=jax.Sha...  60.3 us
    all_to_all x2, blocking collectives, sent_to_all(): return lax.all_to_all(copies, axis, split_axis=0, concat_axis=0, tiled=True)  40 us
    all_to_all x1, blocking collectives, summed_on_arrival(): lax.all_to_all(parts, axis, split_axis=0, concat_axis=0, tiled=True)  34.4 us
    all_gather x1, waiting for transfers between devices, turned_gather(): filled, at, outs = (lax.all_gather(both, axis, axis=0, tiled=True), 0, [])  27.7 us
    all_to_all x1, waiting for transfers between devices, summed_on_arrival(): lax.all_to_all(parts, axis, split_axis=0, concat_axis=0, tiled=True)  26.3 us
    dot_general x1, matrix products, body(): terms = jnp.dot(hidden, whole_down, preferred_element_type=jnp.float32)  11.1 us
    dot_general x1, matrix products, body(): gate = jnp.dot(normed_mid, whole_gate, preferred_element_type=jnp.float32)  5.25 us
    all_to_all x1, starting transfers between devices, summed_on_arrival(): lax.all_to_all(parts, axis, split_axis=0, concat_axis=0, tiled=True)  4.96 us
  transfers between devices with their start and end apart: 2, of which 2 were waited for; matrix products, arithmetic and copies ran while one was open for 6% of the time, Pallas kernels for 25%

profile of v1, /device:TPU:1, one launch (start us, length us, event | category | flops | bytes accessed | tf_op | source)
XLA Modules:
  0.0 244.6 jit_solution(8470443097151900412)
XLA Ops:
  6.5 0.0 copy-start
  6.5 0.0 copy-start.4
  6.5 0.0 copy-start.5
  6.5 0.0 all-gather.2.cloned.1.call-start
  6.5 1.2 copy.49
  7.8 1.1 copy.50
  8.9 1.8 pad_maximum_fusion
  10.7 0.0 all-gather.2.cloned.1.call-update
  10.7 0.1 pad.6.clone
  10.8 0.1 pad.10.clone
  10.9 0.0 copy-done.4
  10.9 0.1 copy.42
  11.1 0.0 copy-done.5
  11.1 0.2 multiply_cosine_fusion
  11.3 0.7 copy.41
  12.1 0.7 copy.40
  12.8 0.8 copy.45
  13.6 0.0 copy-start.1
  13.6 0.8 copy.46
  14.3 0.1 copy.52
  14.4 0.1 copy.53
  14.6 1.2 reshape.112
  15.8 0.0 copy-start.8
  15.8 1.2 fusion.37
  17.0 0.0 copy-start.2
  17.0 0.0 copy-start.3
  17.0 1.1 copy.54
  18.1 1.0 copy.57
  19.1 0.0 copy-done.1
  19.1 0.1 fusion.22
  19.3 1.1 subtract_convert_fusion
  20.4 0.1 maximum_bitcast_fusion.q_ref
  20.5 0.0 copy-done.8
  20.5 0.1 fusion.24
  20.7 0.0 copy-done.2
  20.7 0.0 copy-done.3
  20.7 0.1 maximum_maximum_fusion
  20.8 0.0 copy-start.7
  20.8 60.3 %shard_map.118 = bf16[256,256]{1,0:T(8,128)(2,1)S(1)} custom-call(bf16[2,2,64,640]{3,2,1,0:T(8,128)(2,1)S(1)} %bitcast.18, bf16[2,256,256]{2,1,0:T(8,128)(2,1)S(1)} %maximum_bitcast_fusion.q_ref, bf16[512,256]{1,0:T(8,128)(2,1)S(1)} %bitcast.20, bf16[256,512]{1,0:T(8,128)(2,1)S(1)} %bitcast.19), custom_call_target="tpu_custom_call" | custom-call | flops 20000000000 | bytes 4000000 | tf_op jit(solution)/shard_map/pallas_call | solution.py:315
  81.1 0.1 fusion.30
  81.3 9.6 %all_to_all.21 = f32[8,1,256]{2,1,0:T(1,128)S(1)} all-to-all(f32[8,1,256]{2,1,0:T(1,128)S(1)} %broadcast_in_dim.7), channel_id=1, replica_groups=mesh['sp'=32,'tp'=8] {'tp'}, dimensions={0} | all-to-all | bytes 16384 | tf_op jit(solution)/shard_map/all_to_all | solution.py:40
  90.9 0.0 copy-done
  90.9 0.0 copy-done.7
  91.0 2.1 convolution_convert_fusion
  93.0 5.0 %all-to-all-start.1 = ((bf16[8,32,4096]{2,1,0:T(8,128)(2,1)}), bf16[8,32,4096]{2,1,0:T(8,128)(2,1)}, u32[]{:S(2)}, u32[]{:S(2)}) async-start(bf16[8,32,4096]{2,1,0:T(8,128)(2,1)} %bitcast.21), calls=%async_computation.1 | async-start | bytes 4194304 | tf_op jit(solution)/shard_map/all_to_all | solution.py:55
  98.0 0.0 copy-start.6
  98.0 26.3 %all-to-all-done.1 = bf16[8,32,4096]{2,1,0:T(8,128)(2,1)} async-done(((bf16[8,32,4096]{2,1,0:T(8,128)(2,1)}), bf16[8,32,4096]{2,1,0:T(8,128)(2,1)}, u32[]{:S(2)}, u32[]{:S(2)}) %all-to-all-start.1) | async-done | bytes 2097184 | tf_op jit(solution)/shard_map/all_to_all | solution.py:55
  124.3 2.0 convert_reduce_fusion.1
  126.4 1.2 fusion.25
  127.5 0.0 copy-done.6
  127.5 0.1 fusion.27
  127.7 0.2 broadcast_in_dim.8
  127.9 30.3 %all_to_all.22 = bf16[8,32,4096]{2,1,0:T(8,128)(2,1)} all-to-all(bf16[8,32,4096]{2,1,0:T(8,128)(2,1)S(1)} %broadcast_in_dim.8), channel_id=1, replica_groups=mesh['sp'=32,'tp'=8] {'tp'}, dimensions={0} | all-to-all | bytes 4194304 | tf_op jit(solution)/shard_map/all_to_all | solution.py:40
  158.2 27.7 %all-gather.2.cloned.1.call-done = bf16[4096,2304]{0,1:T(8,128)(2,1)} async-done(((bf16[128,2304]{0,1:T(8,128)(2,1)}), bf16[4096,2304]{0,1:T(8,128)(2,1)}) %all-gather.2.cloned.1.call-update) | async-done | bytes 18874384 | tf_op jit(solution)/shard_map/all_gather | solution.py:30
  185.9 5.2 %fusion.4 = f32[256,768]{1,0:T(8,128)S(1)} fusion(bf16[256,4096]{1,0:T(8,128)(2,1)} %bitcast.22, bf16[4096,2304]{0,1:T(8,128)(2,1)} %all-gather.2.cloned.1.call-done), kind=kOutput, calls=%fused_computation.4 | convolution fusion | flops 1610612736 | bytes 9175040 | tf_op jit(solution)/shard_map/dot_general | solution.py:420
  191.2 11.1 %fusion.6 = bf16[256,4096]{1,0:T(8,128)(2,1)} fusion(bf16[4096,2304]{0,1:T(8,128)(2,1)} %all-gather.2.cloned.1.call-done, bf16[256,4096]{1,0:T(8,128)(2,1)} %bitcast.23, f32[256,768]{1,0:T(8,128)S(1)} %fusion.4), kind=kOutput, calls=%fused_computation.7 | convolution fusion | flops 3223453696 | bytes 17563648 | tf_op jit(solution)/shard_map/dot_general | solution.py:423
  202.3 34.4 %all_to_all.23 = bf16[8,32,4096]{2,1,0:T(8,128)(2,1)S(1)} all-to-all(bf16[8,32,4096]{2,1,0:T(8,128)(2,1)} %bitcast.24), channel_id=1, replica_groups=mesh['sp'=32,'tp'=8] {'tp'}, dimensions={0} | all-to-all | bytes 4194304 | tf_op jit(solution)/shard_map/all_to_all | solution.py:55
  236.7 0.3 convert_reduce_fusion
  237.0 0.8 fusion.28
  (12 shorter events, 0.1 us)
Async XLA Ops:
  6.5 84.4 %copy-start = (bf16[256,4096]{1,0:T(8,128)(2,1)S(1)}, bf16[256,4096]{1,0:T(8,128)(2,1)}, u32[]{:S(2)}) copy-start(bf16[256,4096]{1,0:T(8,128)(2,1)} %param.19) | copy-start | bytes 6291460
  6.5 4.3 %copy-start.4 = (bf16[256,384]{1,0:T(8,128)(2,1)S(1)}, bf16[256,384]{1,0:T(8,128)(2,1)}, u32[]{:S(2)}) copy-start(bf16[256,384]{1,0:T(8,128)(2,1)} %param.13) | copy-start | bytes 589828
  6.5 4.5 %copy-start.5 = (bf16[256,64]{0,1:T(8,128)(2,1)S(1)}, bf16[256,64]{0,1:T(8,128)(2,1)}, u32[]{:S(2)}) copy-start(bf16[256,64]{0,1:T(8,128)(2,1)} %param.15) | copy-start | bytes 98308
  6.5 179.4 %all-gather.2.cloned.1.call-start = ((), (), s32[]{:S(2)}) async-start(), calls=%async_computation.4 | async-start | bytes 19464192 | tf_op jit(solution)/shard_map/all_gather | solution.py:30
  13.6 5.5 %copy-start.1 = (bf16[256,512]{1,0:T(8,128)(2,1)S(1)}, bf16[256,512]{1,0:T(8,128)(2,1)}, u32[]{:S(2)}) copy-start(bf16[256,512]{1,0:T(8,128)(2,1)} %param.14) | copy-start | bytes 786436
  15.8 4.7 %copy-start.8 = (f32[512]{0:T(512)S(1)}, f32[512]{0:T(512)}, u32[]{:S(2)}) copy-start(f32[512]{0:T(512)} %param.16) | copy-start | bytes 6148
  17.0 3.7 %copy-start.2 = (bf16[256,32]{1,0:T(8,128)(2,1)S(1)}, bf16[256,32]{1,0:T(8,128)(2,1)}, u32[]{:S(2)}) copy-start(bf16[256,32]{1,0:T(8,128)(2,1)} %copy.41) | copy-start | bytes 49156
  17.0 3.7 %copy-start.3 = (bf16[256,32]{1,0:T(8,128)(2,1)S(1)}, bf16[256,32]{1,0:T(8,128)(2,1)}, u32[]{:S(2)}) copy-start(bf16[256,32]{1,0:T(8,128)(2,1)} %copy.40) | copy-start | bytes 49156
  20.8 70.2 %copy-start.7 = (f32[256]{0:T(256)S(1)}, f32[256]{0:T(256)}, u32[]{:S(2)}) copy-start(f32[256]{0:T(256)} %param.18) | copy-start | bytes 3076
  93.0 31.3 %all-to-all-start.1 = ((bf16[8,32,4096]{2,1,0:T(8,128)(2,1)}), bf16[8,32,4096]{2,1,0:T(8,128)(2,1)}, u32[]{:S(2)}, u32[]{:S(2)}) async-start(bf16[8,32,4096]{2,1,0:T(8,128)(2,1)} %bitcast.21), calls=%async_computation.1 | async-start | bytes 4194304 | tf_op jit(solution)/shard_map/all_to_all | solution.py:55
  98.0 29.5 %copy-start.6 = (f32[4096]{0:T(1024)S(1)}, f32[4096]{0:T(1024)}, u32[]{:S(2)}) copy-start(f32[4096]{0:T(1024)} %param.20) | copy-start | bytes 49156
Sparse Core Ops, SparseCore 0:
  10.8 175.0 all-gather.1

commit v2 on v0

v2 whole, which is shorter than its diff:
```python
import functools
import math

import jax
import jax.numpy as jnp
from jax import lax
from jax.experimental import pallas as pl
from jax.experimental.pallas import tpu as pltpu
from jax.sharding import PartitionSpec as P

NOPE = 128
ROPE = 64
VDIM = 128
NX = 4
NY = 4
NC = 2
NT = NY * NC
CHUNKS = 2
UNIT = 192

EPSILON = 1e-06
THETA = 10000.0
LOWEST = -1e30
MESH = pl.DeviceIdType.MESH
F32 = jnp.float32
BF16 = jnp.bfloat16


def norm_rows(values, gain):
    wide = values.astype(jnp.float32)
    return wide * lax.rsqrt(jnp.mean(wide * wide, axis=-1, keepdims=True) + EPSILON) * gain


def nt_dot(a, b):
    return lax.dot_general(a, b, (((1,), (1,)), ((), ())), preferred_element_type=F32)


def wide_dot(a, b):
    return jnp.dot(a, b, preferred_element_type=F32)


class Refs:
    def __init__(self, names, values):
        self.__dict__.update(zip(names, values, strict=True))


def remote(src, dst, send, recv, to):
    return pltpu.make_async_remote_copy(
        src_ref=src, dst_ref=dst, send_sem=send, recv_sem=recv, device_id=to, device_id_type=MESH
    )


class Gather4:
    def __init__(self, piece, send, recv, index, plus, minus):
        self.piece, self.send, self.recv, self.index = piece, send, recv, index
        self.plus, self.minus = plus, minus

    def copy(self, way, k, half):
        to = self.plus if way in (0, 2) else self.minus
        ref = self.piece(k, half)
        return remote(ref, ref, self.send.at[self.index, way], self.recv.at[self.index, way], to)

    def start(self):
        self.copy(0, 0, None).start()
        self.copy(1, 0, None).start()

    def near(self, way):
        self.copy(way, 3 if way == 0 else 1, None).wait_recv()
        self.copy(way + 2, 3 if way == 0 else 1, way).start()

    def far(self, half):
        self.copy(half + 2, 2, half).wait_recv()

    def done(self):
        self.copy(0, 0, None).wait_send()
        self.copy(1, 0, None).wait_send()
        self.copy(2, 3, 0).wait_send()
        self.copy(3, 1, 1).wait_send()


class Scatter4:
    def __init__(self, block, half_in, whole_in, send, recv, index, plus, minus):
        self.block, self.half_in, self.whole_in = block, half_in, whole_in
        self.send, self.recv, self.index = send, recv, index
        self.plus, self.minus = plus, minus

    def half(self, h):
        to = self.minus if h == 0 else self.plus
        return remote(
            self.block(2, h), self.half_in.at[h], self.send.at[self.index, h], self.recv.at[self.index, h], to
        )

    def whole(self, h):
        to, k = (self.minus, 3) if h == 0 else (self.plus, 1)
        return remote(
            self.block(k, None),
            self.whole_in.at[h],
            self.send.at[self.index, 2 + h],
            self.recv.at[self.index, 2 + h],
            to,
        )

    def start(self):
        self.half(0).start()
        self.half(1).start()

    def near(self, h):
        self.half(h).wait_recv()
        ref = self.block(3 if h == 0 else 1, h)
        ref[...] = (ref[...].astype(F32) + self.half_in[h].astype(F32)).astype(BF16)
        self.whole(h).start()

    def total(self):
        self.whole(0).wait_recv()
        self.whole(1).wait_recv()
        ref = self.block(0, None)
        return ref[...].astype(F32) + self.whole_in[0].astype(F32) + self.whole_in[1].astype(F32)

    def finish(self):
        self.block(0, None)[...] = self.total().astype(BF16)

    def done(self):
        for h in range(2):
            self.half(h).wait_send()
            self.whole(h).wait_send()


def layer_kernel(nz, names, *values):
    r = Refs(names, values)
    sp, tp = lax.axis_index("sp"), lax.axis_index("tp")
    z, x = sp // NX, lax.rem(sp, NX)
    y, core = tp // NC, lax.rem(tp, NC)
    up = (lax.rem(z + 1, nz) * NX + x, tp)
    down = (lax.rem(z + nz - 1, nz) * NX + x, tp)
    partner = (sp, tp + 1 - 2 * core)
    rows = r.q.shape[1]
    far = nz // 2
    factor = (1.0 / math.sqrt(NOPE + ROPE)) * math.log2(math.e)
    cols = r.resid.shape[1] // NT
    share = rows // NT

    def along_x(k):
        return (z * NX + lax.rem(x + k, NX), tp)

    def along_y(k, other=0):
        to_core = core if other == 0 else 1 - core
        return (sp, lax.rem(y + k, NY) * NC + to_core)

    peers = [up, down, partner]
    peers += [along_x(k) for k in range(1, NX)]
    peers += [along_y(k) for k in range(1, NY)]
    peers += [along_y(k, 1) for k in range(1, NY)]
    barrier = pltpu.get_barrier_semaphore()
    for peer in peers:
        pl.semaphore_signal(barrier, inc=1, device_id=peer, device_id_type=MESH)
    pl.semaphore_wait(barrier, len(peers))

    def ring(src_slot, dst_slot, chunk, to):
        src = r.lat.at[core, chunk] if src_slot is None else r.latbuf.at[src_slot, core, chunk]
        dst = r.latbuf.at[dst_slot, core, chunk]
        return remote(src, dst, r.ring_send.at[dst_slot, chunk], r.ring_recv.at[dst_slot, chunk], to)

    def pair(slot, chunk, side):
        ref = r.latbuf.at[slot, side, chunk]
        return remote(ref, ref, r.pair_send.at[slot, chunk], r.pair_recv.at[slot, chunk], partner)

    def q_copy(k):
        return remote(r.q, r.qbuf.at[x], r.q_send.at[k], r.q_recv.at[k], along_x(k))

    def weight_copies(k):
        to = lax.rem(x + k, NX)
        return [
            remote(r.gu.at[to], r.gubuf.at[z, x], r.wx_send.at[k, 0], r.wx_recv.at[k, 0], along_x(k)),
            remote(r.dn.at[to], r.dnbuf.at[z, x], r.wx_send.at[k, 1], r.wx_recv.at[k, 1], along_x(k)),
        ]

    def ow_copy(i):
        k, other = i // 2, i % 2
        to = along_y(k, other)
        src = r.ow.at[:, pl.ds(pl.multiple_of(to[1] * cols, cols), cols)]
        return remote(src, r.owbuf.at[tp], r.ow_send.at[i], r.ow_recv.at[i], to)

    for chunk in range(CHUNKS):
        ring(None, 1, chunk, up).start()
        ring(None, far + 1, chunk, down).start()
    own_cols = pl.ds(pl.multiple_of(tp * cols, cols), cols)
    local = [
        pltpu.make_async_copy(r.lat, r.latbuf.at[0], r.local_sem.at[0]),
        pltpu.make_async_copy(r.q, r.qbuf.at[x], r.local_sem.at[1]),
        pltpu.make_async_copy(r.gu.at[x], r.gubuf.at[z, x], r.local_sem.at[2]),
        pltpu.make_async_copy(r.dn.at[x], r.dnbuf.at[z, x], r.local_sem.at[3]),
        pltpu.make_async_copy(r.ow.at[:, own_cols], r.owbuf.at[tp], r.local_sem.at[4]),
        pltpu.make_async_copy(r.resid.at[:, own_cols], r.residbuf, r.local_sem.at[5]),
    ]
    for copy in local:
        copy.start()
    for k in range(1, NX):
        q_copy(k).start()
    for k in range(1, NX):
        for copy in weight_copies(k):
            copy.start()
    for i in range(1, NT):
        ow_copy(i).start()

    r.stat_m[...] = jnp.full(r.stat_m.shape, LOWEST, F32)
    r.stat_l[...] = jnp.zeros(r.stat_l.shape, F32)
    r.acc[...] = jnp.zeros(r.acc.shape, F32)

    def piece(slot, diagonal):
        lat = r.latbuf[slot].reshape(rows, r.lat.shape[-1])
        wide = r.wk.shape[0]
        compressed, key_rot = lat[:, :wide], lat[:, wide:]
        keys = wide_dot(compressed, r.wk[...]).astype(BF16)
        values = nt_dot(r.wv[...], compressed).astype(BF16)
        for h in range(2):
            key = jnp.concatenate([keys[:, h * NOPE : (h + 1) * NOPE], key_rot], axis=1)
            value = values[h * VDIM : (h + 1) * VDIM]
            for b in range(NX):
                at = pl.ds(b * rows, rows)
                scores = nt_dot(key, r.qbuf[b, h]) * factor
                if diagonal:
                    key_at = x * rows + lax.broadcasted_iota(jnp.int32, scores.shape, 0)
                    query_at = b * rows + lax.broadcasted_iota(jnp.int32, scores.shape, 1)
                    allowed = key_at <= query_at
                    scores = jnp.where(allowed, scores, LOWEST)
                old = r.stat_m[h, :, at]
                new = jnp.maximum(old, jnp.max(scores, axis=0, keepdims=True))
                weights = jnp.exp2(scores - new)
                if diagonal:
                    weights = jnp.where(allowed, weights, 0.0)
                shrink = jnp.exp2(old - new)
                r.stat_m[h, :, at] = new
                r.stat_l[h, :, at] = r.stat_l[h, :, at] * shrink + jnp.sum(
                    weights, axis=0, keepdims=True
                )
                r.acc[h, :, at] = r.acc[h, :, at] * shrink + wide_dot(value, weights.astype(BF16))

    for copy in local[:2]:
        copy.wait()
    for k in range(1, NX):
        q_copy(k).wait_recv()
    piece(0, True)

    def arrive(slot, forward_to, to):
        for chunk in range(CHUNKS):
            ring(None, slot, chunk, to).wait_recv()
            if forward_to is not None:
                ring(slot, forward_to, chunk, to).start()
            pair(slot, chunk, core).start()

    def use(slot, needed):
        for chunk in range(CHUNKS):
            pair(slot, chunk, 1 - core).wait_recv()

        @pl.when(needed)
        def _():
            piece(slot, False)

    def both(d):
        def one(i, carry):
            slot = jnp.where(i == 0, d, far + d)
            source = jnp.where(i == 0, z - d, z + d - nz)
            use(slot, source >= 0)
            return carry

        return one

    def hop(d, way, part):
        of = lax.rem(z - (d - 1) + nz, nz) if way == 0 else lax.rem(z + d - 1, nz)
        ref = (r.gubuf if part == 0 else r.dnbuf).at[of]
        to = up if way == 0 else down
        return remote(ref, ref, r.hop_send.at[d, way, part], r.hop_recv.at[d, way, part], to)

    def hop_in(d, way, part):
        of = lax.rem(z - d + nz, nz) if way == 0 else lax.rem(z + d, nz)
        ref = (r.gubuf if part == 0 else r.dnbuf).at[of]
        to = up if way == 0 else down
        return remote(ref, ref, r.hop_send.at[d, way, part], r.hop_recv.at[d, way, part], to)

    def in_hop(d):
        return [(way, part) for part in range(2) for way in range(2) if d < far or way == part]

    def hop_first():
        for k in range(1, NX):
            for copy in weight_copies(k):
                copy.wait_recv()
        local[2].wait()
        local[3].wait()
        for way, part in in_hop(1):
            hop(1, way, part).start()

    def hop_on(d):
        for way, part in in_hop(d):
            hop_in(d, way, part).wait_recv()
            if d < far and (way, part) in in_hop(d + 1):
                hop(d + 1, way, part).start()

    for d in range(1, far + 1):
        arrive(d, d + 1 if d < far else None, up)
        if d < far:
            arrive(far + d, far + d + 1 if d < far - 1 else None, down)
        if d == far:
            hop_first()
        if d > 1:
            lax.fori_loop(0, 2, both(d - 1), 0)
    use(far, z - far >= 0)

    for b in range(NX):
        at = pl.ds(b * rows, rows)
        for h in range(2):
            total = r.stat_l[h, :, at]
            inverse = jnp.where(total > 0.0, 1.0 / jnp.where(total > 0.0, total, 1.0), 0.0)
            r.osend[b, h * VDIM : (h + 1) * VDIM] = (r.acc[h, :, at] * inverse).astype(BF16)
            r.ssend[b, h : h + 1] = r.stat_m[h, :, at]
            r.ssend[b, 2 + h : 3 + h] = total

    def o_copy(k):
        to = lax.rem(x + k, NX)
        return remote(r.osend.at[to], r.orecv.at[k], r.o_send.at[k], r.o_recv.at[k], along_x(k))

    def s_copy(k):
        to = lax.rem(x + k, NX)
        return remote(r.ssend.at[to], r.srecv.at[k], r.s_send.at[k], r.s_recv.at[k], along_x(k))

    for k in range(1, NX):
        s_copy(k).start()
        o_copy(k).start()
    for k in range(1, NX):
        s_copy(k).wait_recv()
        o_copy(k).wait_recv()
    width = 2 * VDIM
    stats = [r.ssend[x]] + [r.srecv[k] for k in range(1, NX)]
    for h in range(2):
        outs = [r.osend[x, h * VDIM : (h + 1) * VDIM]] + [
            r.orecv[k, h * VDIM : (h + 1) * VDIM] for k in range(1, NX)
        ]
        top = functools.reduce(jnp.maximum, [s[h : h + 1] for s in stats])
        shares = [s[2 + h : 3 + h] * jnp.exp2(s[h : h + 1] - top) for s in stats]
        inverse = 1.0 / sum(shares)
        mixed = sum(o.astype(F32) * (w * inverse) for o, w in zip(outs, shares))
        at = pl.ds(pl.multiple_of(tp * width + h * VDIM, VDIM), VDIM)
        r.att[:, at] = jnp.transpose(mixed).astype(BF16)

    def att_piece(own_core):
        def ref(k, half):
            of = lax.rem(y + k, NY) * NC + own_core
            where = pl.ds(pl.multiple_of(of * width, width), width)
            at = pl.ds(0, rows) if half is None else pl.ds(half * (rows // 2), rows // 2)
            return r.att.at[at, where]

        return ref

    ga = Gather4(att_piece(core), r.ga_send, r.ga_recv, 0, along_y(1), along_y(3))

    def swap(piece, send, recv, index):
        k, half = ((0, None), (3, None), (1, None), (2, 0), (2, 1))[index]
        mine, theirs = piece(core)(k, half), piece(1 - core)(k, half)
        out = functools.partial(remote, mine, mine, send.at[index], recv.at[index], partner)
        come = functools.partial(remote, theirs, theirs, send.at[index], recv.at[index], partner)
        return out, come

    swaps = [swap(att_piece, r.sa_send.at[0], r.sa_recv.at[0], i) for i in range(5)]
    ga.start()
    swaps[0][0]().start()
    ga.near(0)
    swaps[1][0]().start()
    ga.near(1)
    swaps[2][0]().start()
    ga.far(0)
    swaps[3][0]().start()
    ga.far(1)
    swaps[4][0]().start()
    for i in range(1, NT):
        ow_copy(i).wait_recv()
    local[4].wait()
    local[5].wait()
    hop_on(1)
    for out, come in swaps:
        come().wait_recv()

    att = r.att[...]
    att_wide = att.astype(F32)
    scale = lax.rsqrt(jnp.mean(att_wide * att_wide, axis=1, keepdims=True) + EPSILON)
    attn_sum = wide_dot(att, r.owbuf[...].reshape(att.shape[1], cols)) * scale
    r.mid[x, :, own_cols] = (r.residbuf[...].astype(F32) + attn_sum).astype(BF16)

    def mid_piece(axis, at_x, at_y, own_core, first):
        def ref(k, half):
            of_x = lax.rem(x + at_x + (k if axis == 0 else 0), NX)
            of_y = lax.rem(y + at_y + (k if axis == 1 else 0), NY)
            where = pl.ds(pl.multiple_of((of_y * NC + own_core) * cols, cols), cols)
            quarter = rows // 4
            at = pl.ds(first * 2 * quarter, 2 * quarter)
            if half is not None:
                at = pl.ds((first * 2 + half) * quarter, quarter)
            return r.mid.at[of_x, at, where]

        return ref

    def plane_ring(index, axis, at_x, at_y, first):
        piece_of = functools.partial(lambda c: mid_piece(axis, at_x, at_y, c, first))
        plus, minus = (along_x(1), along_x(3)) if axis == 0 else (along_y(1), along_y(3))
        g = Gather4(piece_of(core), r.gm_send, r.gm_recv, index, plus, minus)
        return g, [swap(piece_of, r.sm_send.at[index], r.sm_recv.at[index], i) for i in range(5)]

    offsets = (0, 3, 1, 2)
    first_rings = [plane_ring(0, 0, 0, 0, 0), plane_ring(1, 1, 0, 0, 1)]
    second_rings = [
        [plane_ring(2 + i, 1, k, 0, 0), plane_ring(6 + i, 0, 0, k, 1)] for i, k in enumerate(offsets)
    ]
    for g, s in first_rings:
        g.start()
        s[0][0]().start()
    for g, s in second_rings[0]:
        g.start()
    for way in range(2):
        for i, (g, s) in enumerate(first_rings):
            g.near(way)
            second_rings[1 + way][i][0].start()
            s[1 + way][0]().start()
    for way in range(2):
        for g, s in second_rings[0]:
            g.near(way)
            s[1 + way][0]().start()
    for i, (g, s) in enumerate(first_rings):
        for half in range(2):
            g.far(half)
            s[3 + half][0]().start()
        second_rings[3][i][0].start()
    hop_on(2)
    for j in range(1, 4):
        for way in range(2):
            for g, s in second_rings[j]:
                g.near(way)
                s[1 + way][0]().start()
        for half in range(2):
            for g, s in second_rings[j - 1]:
                g.far(half)
                s[3 + half][0]().start()
        if j == 2 and far > 3:
            hop_on(3)
    for half in range(2):
        for g, s in second_rings[3]:
            g.far(half)
            s[3 + half][0]().start()
    if far == 2:
        pass
    else:
        hop_on(far)
    rings = first_rings + [pair_of for both_of in second_rings for pair_of in both_of]
    for i, (g, s) in enumerate(rings):
        for j, (out, come) in enumerate(s):
            if j > 0 or i < 2:
                come().wait_recv()

    def mixer(b, carry):
        squares = jnp.zeros((rows, 128), F32)
        for j in range(r.mid.shape[2] // 128):
            v = r.mid[b, :, j * 128 : (j + 1) * 128].astype(F32)
            squares = squares + v * v
        mean = jnp.sum(squares, axis=1, keepdims=True) / r.mid.shape[2]
        row_scale = lax.rsqrt(mean + EPSILON)
        mid = r.mid[b]
        gu = wide_dot(mid, r.gubuf[...].reshape(mid.shape[1], 2 * UNIT)) * row_scale
        gate, mixed_tile, upward = gu[:, :128], gu[:, 128:256], gu[:, 256:]
        first = gate / (1.0 + jnp.exp(-gate)) * upward
        second = (mixed_tile / (1.0 + jnp.exp(-mixed_tile)))[:, :64] * mixed_tile[:, 64:]
        hidden = jnp.concatenate([first, second], axis=1).astype(BF16)
        n = r.dnbuf.shape[-1]
        for zz in range(nz):
            w = jnp.concatenate([r.dnbuf[zz, i] for i in range(NX)], axis=1)
            terms = wide_dot(hidden, w).astype(BF16).reshape(NY, NC, share, NX * n)
            for c in range(NC):
                r.part[c, b, :, :, zz * NX * n : (zz + 1) * NX * n] = terms[:, c]
        core_copy(b).start()
        return carry

    def core_copy(b):
        return remote(r.part.at[1 - core, b], r.pairbuf.at[b], r.pc_send.at[b], r.pc_recv.at[b], partner)

    lax.fori_loop(0, NX, mixer, 0)

    def core_sum(b, carry):
        core_copy(b).wait_recv()
        for i in range(NY):
            ref = r.part.at[core, b, i]
            ref[...] = (ref[...].astype(F32) + r.pairbuf[b, i].astype(F32)).astype(BF16)
        return carry

    lax.fori_loop(0, NX, core_sum, 0)

    depth = r.part.shape[-1] // 2

    def block(axis, of_x, of_y, first):
        def ref(k, half):
            bx = lax.rem(of_x + (k if axis == 0 else 0), NX)
            by = lax.rem(of_y + (k if axis == 1 else 0), NY)
            at = pl.ds(first * depth, depth)
            if half is not None:
                at = pl.ds(first * depth + half * (depth // 2), depth // 2)
            return r.part.at[core, bx, by, :, at]

        return ref

    def scatter(index, axis, of_x, of_y, first):
        plus, minus = (along_x(1), along_x(3)) if axis == 0 else (along_y(1), along_y(3))
        return Scatter4(
            block(axis, of_x, of_y, first),
            r.half_in.at[index],
            r.whole_in.at[index],
            r.rs_send,
            r.rs_recv,
            index,
            plus,
            minus,
        )

    order = (1, 3, 2, 0)
    steps = [
        [scatter(i, 1, x + k, y, 0), scatter(4 + i, 0, x, y + k, 1)] for i, k in enumerate(order)
    ]
    ends = [scatter(8, 0, x, y, 0), scatter(9, 1, x, y, 1)]
    for both_of in steps:
        for s in both_of:
            s.start()
    for both_of in steps:
        for s in both_of:
            s.near(0)
            s.near(1)
    for j, both_of in enumerate(steps):
        for s in both_of:
            s.finish()
        if j == 2:
            for s in ends:
                s.start()
    for s in ends:
        s.near(0)
        s.near(1)
    own_rows = pl.ds(pl.multiple_of(tp * share, share), share)
    for first, s in enumerate(ends):
        at = slice(first * depth, (first + 1) * depth)
        r.out[:, at] = (s.total() + r.mid[x, own_rows, at].astype(F32)).astype(BF16)

    for k in range(1, NX):
        q_copy(k).wait_send()
        o_copy(k).wait_send()
        s_copy(k).wait_send()
        for copy in weight_copies(k):
            copy.wait_send()
    for i in range(1, NT):
        ow_copy(i).wait_send()
    for slot in range(1, nz):
        for chunk in range(CHUNKS):
            ring(None, slot, chunk, up).wait_send()
            pair(slot, chunk, core).wait_send()
    for d in range(1, far + 1):
        for way, part in in_hop(d):
            hop(d, way, part).wait_send()
    ga.done()
    for out, come in swaps:
        out().wait_send()
    for i, (g, s) in enumerate(rings):
        g.done()
        for j, (out, come) in enumerate(s):
            if j > 0 or i < 2:
                out().wait_send()
    for b in range(NX):
        core_copy(b).wait_send()
    for both_of in [*steps, ends]:
        for s in both_of:
            s.done()


def layer(lat, q, wk, wv, gu, dn, ow, resid):
    nz = lax.axis_size("sp") // NX
    rows, wide = lat.shape
    dim = resid.shape[1]
    share = rows // NT
    cols = dim // NT
    lat = lat.reshape(NC, CHUNKS, rows // NC // CHUNKS, wide)
    vmem = pl.BlockSpec(memory_space=pltpu.VMEM)
    anywhere = pl.BlockSpec(memory_space=pl.ANY)
    inputs = {
        "lat": (lat, vmem),
        "q": (q, vmem),
        "wk": (wk, vmem),
        "wv": (wv, vmem),
        "gu": (gu, anywhere),
        "dn": (dn, anywhere),
        "ow": (ow, anywhere),
        "resid": (resid, anywhere),
    }
    buffers = {
        "latbuf": ((nz, *lat.shape), BF16),
        "qbuf": ((NX, *q.shape), BF16),
        "acc": ((2, VDIM, NX * rows), F32),
        "stat_m": ((2, 1, NX * rows), F32),
        "stat_l": ((2, 1, NX * rows), F32),
        "osend": ((NX, 2 * VDIM, rows), BF16),
        "orecv": ((NX, 2 * VDIM, rows), BF16),
        "ssend": ((NX, 8, rows), F32),
        "srecv": ((NX, 8, rows), F32),
        "gubuf": ((nz, *gu.shape), BF16),
        "dnbuf": ((nz, *dn.shape), BF16),
        "owbuf": ((NT, ow.shape[0], cols), BF16),
        "residbuf": ((rows, cols), BF16),
        "att": ((rows, NT * 2 * VDIM), BF16),
        "mid": ((NX, rows, dim), BF16),
        "part": ((NC, NX, NY, share, dim), BF16),
        "pairbuf": ((NX, NY, share, dim), BF16),
        "half_in": ((10, 2, share, dim // 4), BF16),
        "whole_in": ((10, 2, share, dim // 2), BF16),
    }
    semaphores = {
        "local_sem": (6,),
        "ring_send": (nz, CHUNKS),
        "ring_recv": (nz, CHUNKS),
        "pair_send": (nz, CHUNKS),
        "pair_recv": (nz, CHUNKS),
        "q_send": (NX,),
        "q_recv": (NX,),
        "wx_send": (NX, 2),
        "wx_recv": (NX, 2),
        "ow_send": (NT,),
        "ow_recv": (NT,),
        "hop_send": (nz, 2, 2),
        "hop_recv": (nz, 2, 2),
        "o_send": (NX,),
        "o_recv": (NX,),
        "s_send": (NX,),
        "s_recv": (NX,),
        "ga_send": (1, 4),
        "ga_recv": (1, 4),
        "sa_send": (1, 5),
        "sa_recv": (1, 5),
        "gm_send": (10, 4),
        "gm_recv": (10, 4),
        "sm_send": (10, 5),
        "sm_recv": (10, 5),
        "pc_send": (NX,),
        "pc_recv": (NX,),
        "rs_send": (10, 4),
        "rs_recv": (10, 4),
    }
    names = [*inputs, "out", *buffers, *semaphores]
    return pl.pallas_call(
        functools.partial(layer_kernel, nz, names),
        out_shape=jax.ShapeDtypeStruct((share, dim), BF16),
        in_specs=[spec for _, spec in inputs.values()],
        out_specs=vmem,
        scratch_shapes=[pltpu.VMEM(*b) for b in buffers.values()]
        + [pltpu.SemaphoreType.DMA(s) for s in semaphores.values()],
        compiler_params=pltpu.CompilerParams(
            collective_id=0, has_side_effects=True, vmem_limit_bytes=62 * 1024 * 1024
        ),
    )(*[array for array, _ in inputs.values()])


def turned(values, cosine, sine):
    half = values.shape[-1] // 2
    first, second = values[..., :half], values[..., half:]
    return jnp.concatenate(
        [first * cosine - second * sine, first * sine + second * cosine], axis=-1
    )


def body(
    resid,
    queries,
    latent,
    rope_key,
    lat_gain,
    kv_weight,
    out_gain,
    out_weight,
    ffn_gain,
    gate_weight,
    up_weight,
    down_weight,
):
    rows = latent.shape[0]
    sp = lax.axis_index("sp")
    heads_here = queries.shape[1] // (NOPE + ROPE)
    places = (sp * rows + jnp.arange(rows, dtype=jnp.int32)).astype(F32)
    half = ROPE // 2
    inverse = THETA ** (-jnp.arange(half, dtype=F32) / half)
    angle = places[:, None] * inverse
    cosine, sine = jnp.cos(angle), jnp.sin(angle)
    pad = jnp.zeros((rows, NOPE - ROPE), BF16)
    key_rot = turned(rope_key.astype(F32), cosine, sine).astype(BF16)
    normed = norm_rows(latent, lat_gain).astype(BF16)
    lat = jnp.concatenate([normed, key_rot, pad], axis=1)
    query = queries.reshape(rows, heads_here, NOPE + ROPE)
    query_rot = turned(
        query[:, :, NOPE:].astype(F32), cosine[:, None], sine[:, None]
    ).astype(BF16)
    full = jnp.concatenate(
        [query[:, :, :NOPE], query_rot, jnp.broadcast_to(pad[:, None], (rows, heads_here, NOPE - ROPE))],
        axis=2,
    )
    full = jnp.transpose(full, (1, 0, 2))
    weight = kv_weight.reshape(kv_weight.shape[0], heads_here, NOPE + VDIM)
    wk = weight[:, :, :NOPE].reshape(-1, heads_here * NOPE)
    wv = jnp.transpose(weight[:, :, NOPE:].reshape(-1, heads_here * VDIM))
    depth = gate_weight.shape[0]
    gain = lax.dynamic_slice_in_dim(ffn_gain, sp * depth, depth)[:, None]
    gate = (gate_weight.astype(F32) * gain).astype(BF16)
    upward = (up_weight.astype(F32) * gain).astype(BF16)
    gu = jnp.stack(
        [
            jnp.concatenate(
                [
                    gate[:, i * UNIT : i * UNIT + 128],
                    gate[:, i * UNIT + 128 : (i + 1) * UNIT],
                    upward[:, i * UNIT + 128 : (i + 1) * UNIT],
                    upward[:, i * UNIT : i * UNIT + 128],
                ],
                axis=1,
            )
            for i in range(NX)
        ]
    )
    dn = down_weight.reshape(NX, UNIT, down_weight.shape[1])
    ow = (out_weight.astype(F32) * out_gain[:, None]).astype(BF16)
    return layer(lat, full, wk, wv, gu, dn, ow, resid)


def solution(mesh):
    placed = (
        P("sp", None),
        P("sp", "tp"),
        P("sp", None),
        P("sp", None),
        P(),
        P(None, "tp"),
        P("tp"),
        P("tp", None),
        P(),
        P("sp", "tp"),
        P("sp", "tp"),
        P("tp", "sp"),
    )
    return jax.shard_map(
        body, mesh=mesh, in_specs=placed, out_specs=P(("sp", "tp"), None), check_vma=False
    )
```

time: 341 us -> 159 us (0.47)
  waiting for transfers between devices: 147 us -> 0 us
  Pallas kernels: 0 us -> 144 us
  blocking collectives: 75.1 us -> 0 us
  matrix products: 53.1 us -> 0 us
  local copies, waits for them, and re-layouts: 25 us -> 6.78 us
  other arithmetic: 20.6 us -> 7.11 us
  between operations: 13.5 us -> 0.19 us
  starting transfers between devices: 4.9 us -> 0 us
    pallas_call x0 -> x1, Pallas kernels: none -> 144 us  [layer(): pl.pallas_call(functools.partial(layer_kernel, nz, names), out_shape=jax....]
    all_gather x2 -> x0, waiting for transfers between devices: 121 us -> none  [the longest x1 106 us: side_by_side(): lax.all_gather(both, axis, axis=dim, tiled=True)]
    all_to_all x3 -> x0, blocking collectives: 75.1 us -> none  [the longest x2 40.6 us: sent_to_all(): return lax.all_to_all(copies, axis, split_axis=0, concat_axis=0, tiled=True)]
    dot_general x7 -> x0, matrix products: 53.1 us -> none  [the longest x1 15.2 us: accumulate(): jnp.einsum('qhd,khd->hqk', query_nope, key_value[:, :, :NOPE], preferred_...]
    all_to_all x1 -> x0, waiting for transfers between devices: 26.3 us -> none  [summed_on_arrival(): lax.all_to_all(parts, axis, split_axis=0, concat_axis=0, tiled=True)]
    another operation x4 -> x2, local copies, waits for them, and re-layouts: 13.5 us -> 0.24 us
    reduce_sum x5 -> x0, other arithmetic: 10.9 us -> none  [the longest x1 8.52 us: accumulate(): running_sum = jnp.sum(weights, axis=-1)]
    split x1 -> x0, local copies, waits for them, and re-layouts: 7.9 us -> none  [side_by_side(): jnp.split(lax.all_gather(both, axis, axis=dim, tiled=True), ends, axis=al...]
  transfers between devices with their start and end apart: 3 -> 0, of which waited for: 3 -> 0; matrix products, arithmetic and copies ran while one was open for 23% -> 0% of each run, Pallas kernels for 0% -> 0%
where the time goes in v2:
time: 159 us; the launch traced here: 158 us
  Pallas kernels  144 us (91%)
  other arithmetic  7.11 us (4%)
  local copies, waits for them, and re-layouts  6.78 us (4%)
    pallas_call x1, Pallas kernels, layer(): pl.pallas_call(functools.partial(layer_kernel, nz, names), out_shape=jax....  144 us
    unnamed x20, local copies, waits for them, and re-layouts  4.64 us

profile of v2, /device:TPU:1, one launch (start us, length us, event | category | flops | bytes accessed | tf_op | source)
XLA Modules:
  0.0 158.2 jit_solution(2169842614824198147)
XLA Ops:
  0.0 0.8 dynamic_slice.3
  0.8 0.1 pad.19.clone
  0.9 1.1 fusion
  1.9 0.0 copy-start.1
  2.0 0.0 copy-start.5
  2.0 0.1 pad.23.clone
  2.1 0.8 convert_element_type.41
  2.8 0.2 multiply_cosine_fusion
  3.0 0.1 copy.19
  3.1 0.1 copy.18
  3.3 0.1 copy.23
  3.4 0.1 copy.24
  3.5 1.1 copy.20
  4.5 0.0 copy-start.3
  4.6 0.0 copy-start.4
  4.6 0.1 copy.26
  4.7 0.1 copy.27
  4.9 0.2 subtract_convert_fusion
  5.0 0.8 maximum_bitcast_fusion.values_1_
  5.9 0.0 copy-done.1
  5.9 0.0 copy-done.5
  5.9 0.1 fusion.2
  6.0 0.0 copy-start.2
  6.0 0.8 maximum_maximum_fusion
  6.8 0.0 copy-done.3
  6.8 0.0 copy-done.4
  6.8 0.1 multiply_convert_fusion.2
  7.0 0.1 fusion.4
  7.1 0.1 fusion.6
  7.2 0.1 fusion.5
  7.3 0.1 maximum_bitcast_fusion.1
  7.4 0.0 copy-start
  7.4 0.0 copy-start.6
  7.4 0.1 maximum_bitcast_fusion.3
  7.5 0.8 pad_maximum_fusion.values_4_
  8.4 0.0 copy-done.2
  8.4 0.1 reshape.89
  8.5 0.4 fusion.3
  8.9 0.9 copy.28
  9.7 0.8 copy.31
  10.5 0.0 copy-done
  10.5 0.0 copy-done.6
  10.5 1.9 %multiply_convert_fusion.values_6_ = bf16[256,4096]{1,0:T(8,128)(2,1)} fusion(bf16[256,4096]{1,0:T(8,128)(2,1)S(1)} %copy-done, f32[256]{0:T(256)S(1)} %copy-done.6), kind=kLoop, calls=%fused_computation | loop fusion | flops 3145728 | bytes 4195328 | tf_op jit(solution)/shard_map/convert_element_type | solution.py:724
  12.4 144.1 %shard_map.118 = bf16[32,4096]{1,0:T(8,128)(2,1)} custom-call(bf16[2,2,64,640]{3,2,1,0:T(8,128)(2,1)} %bitcast.20, bf16[2,256,256]{2,1,0:T(8,128)(2,1)} %maximum_bitcast_fusion.values_1_, bf16[512,256]{1,0:T(8,128)(2,1)} %bitcast.22, bf16[256,512]{1,0:T(8,128)(2,1)} %bitcast.21, bf16[4,128,384]{2,1,0:T(8,128)(2,1)} %pad_maximum_fusion.values_4_, ...), custom_call_target="tpu_custom_call" | custom-call | tf_op jit(solution)/shard_map/pallas_call | solution.py:646
  156.5 1.7 %copy.33 = bf16[32,4096]{1,0:T(8,128)(2,1)} copy(bf16[32,4096]{1,0:T(8,128)(2,1)} %shard_map.118) | data formatting | bytes 524288
  (7 shorter events, 0.1 us)
Async XLA Ops:
  1.9 3.9 %copy-start.1 = (bf16[256,512]{1,0:T(8,128)(2,1)S(1)}, bf16[256,512]{1,0:T(8,128)(2,1)}, u32[]{:S(2)}) copy-start(bf16[256,512]{1,0:T(8,128)(2,1)} %param.14) | copy-start | bytes 786436
  2.0 3.9 %copy-start.5 = (f32[512]{0:T(512)S(1)}, f32[512]{0:T(512)}, u32[]{:S(2)}) copy-start(f32[512]{0:T(512)} %param.16) | copy-start | bytes 6148
  4.5 2.3 %copy-start.3 = (bf16[128,768]{1,0:T(8,128)(2,1)S(1)}, bf16[128,768]{1,0:T(8,128)(2,1)}, u32[]{:S(2)}) copy-start(bf16[128,768]{1,0:T(8,128)(2,1)} %param.21) | copy-start | bytes 589828
  4.6 2.3 %copy-start.4 = (bf16[128,768]{1,0:T(8,128)(2,1)S(1)}, bf16[128,768]{1,0:T(8,128)(2,1)}, u32[]{:S(2)}) copy-start(bf16[128,768]{1,0:T(8,128)(2,1)} %param.22) | copy-start | bytes 589828
  6.0 2.4 %copy-start.2 = (bf16[512,512]{1,0:T(8,128)(2,1)S(1)}, bf16[512,512]{1,0:T(8,128)(2,1)}, u32[]{:S(2)}) copy-start(bf16[512,512]{1,0:T(8,128)(2,1)} %param.17) | copy-start | bytes 1572868
  7.4 3.1 %copy-start = (bf16[256,4096]{1,0:T(8,128)(2,1)S(1)}, bf16[256,4096]{1,0:T(8,128)(2,1)}, u32[]{:S(2)}) copy-start(bf16[256,4096]{1,0:T(8,128)(2,1)} %param.19) | copy-start | bytes 6291460
  7.4 3.1 %copy-start.6 = (f32[256]{0:T(256)S(1)}, f32[256]{0:T(256)}, u32[]{:S(2)}) copy-start(f32[256]{0:T(256)} %param.18) | copy-start | bytes 3076

commit v3 on v2

--- a/solution.py
+++ b/solution.py
@@ -3,6 +3,7 @@
 
 import jax
 import jax.numpy as jnp
+import numpy as np
 from jax import lax
 from jax.experimental import pallas as pl
 from jax.experimental.pallas import tpu as pltpu
@@ -27,8 +28,20 @@
 
 
 def norm_rows(values, gain):
-    wide = values.astype(jnp.float32)
+    wide = values.astype(F32)
     return wide * lax.rsqrt(jnp.mean(wide * wide, axis=-1, keepdims=True) + EPSILON) * gain
+
+
+def column(row):
+    return jnp.transpose(jnp.broadcast_to(row, (128, row.shape[1])))[:, :1]
+
+
+def turned(values, cosine, sine):
+    half = values.shape[-1] // 2
+    first, second = values[:, :half], values[:, half:]
+    return jnp.concatenate(
+        [first * cosine - second * sine, first * sine + second * cosine], axis=1
+    )
 
 
 def nt_dot(a, b):
@@ -133,10 +146,11 @@
     up = (lax.rem(z + 1, nz) * NX + x, tp)
     down = (lax.rem(z + nz - 1, nz) * NX + x, tp)
     partner = (sp, tp + 1 - 2 * core)
-    rows = r.q.shape[1]
+    rows = r.latent.shape[0]
     far = nz // 2
     factor = (1.0 / math.sqrt(NOPE + ROPE)) * math.log2(math.e)
-    cols = r.resid.shape[1] // NT
+    dim = r.resid.shape[1]
+    cols = dim // NT
     share = rows // NT
 
     def along_x(k):
@@ -153,10 +167,36 @@
     barrier = pltpu.get_barrier_semaphore()
     for peer in peers:
         pl.semaphore_signal(barrier, inc=1, device_id=peer, device_id_type=MESH)
+
+    own_cols = pl.ds(pl.multiple_of(tp * cols, cols), cols)
+    local = [
+        pltpu.make_async_copy(r.ow, r.owstage, r.local_sem.at[0]),
+        pltpu.make_async_copy(r.dn.at[x], r.dnbuf.at[z, x], r.local_sem.at[1]),
+        pltpu.make_async_copy(r.resid.at[:, own_cols], r.residbuf, r.local_sem.at[2]),
+        pltpu.make_async_copy(r.gustage.at[x], r.gubuf.at[z, x], r.local_sem.at[3]),
+        pltpu.make_async_copy(r.owstage.at[:, own_cols], r.owbuf.at[tp], r.local_sem.at[4]),
+    ]
+    for copy in local[:3]:
+        copy.start()
+
+    half = ROPE // 2
+    base, step = r.first_turn[pl.ds(sp, 1), :], r.row_turn[...]
+    base_cos, base_sin = base[:, :half], base[:, half:]
+    step_cos, step_sin = step[:, :half], step[:, half:]
+    cosine = base_cos * step_cos - base_sin * step_sin
+    sine = base_sin * step_cos + base_cos * step_sin
+    key_rot = turned(r.rope_key[...].astype(F32), cosine, sine)
+    lat = jnp.concatenate([norm_rows(r.latent[...], r.lat_gain[...]), key_rot, key_rot], axis=1)
+    r.latbuf[0] = lat.astype(BF16).reshape(r.latbuf.shape[1:])
+    query = r.queries[...].astype(F32)
+    one = NOPE + ROPE
+    parts = [query[:, h * one : h * one + NOPE] for h in range(2)]
+    parts += [turned(query[:, h * one + NOPE : (h + 1) * one], cosine, sine) for h in range(2)]
+    r.qbuf[x] = jnp.concatenate(parts, axis=1).astype(BF16)
     pl.semaphore_wait(barrier, len(peers))
 
     def ring(src_slot, dst_slot, chunk, to):
-        src = r.lat.at[core, chunk] if src_slot is None else r.latbuf.at[src_slot, core, chunk]
+        src = r.latbuf.at[src_slot, core, chunk]
         dst = r.latbuf.at[dst_slot, core, chunk]
         return remote(src, dst, r.ring_send.at[dst_slot, chunk], r.ring_recv.at[dst_slot, chunk], to)
 
@@ -164,41 +204,55 @@
         ref = r.latbuf.at[slot, side, chunk]
         return remote(ref, ref, r.pair_send.at[slot, chunk], r.pair_recv.at[slot, chunk], partner)
 
-    def q_copy(k):
-        return remote(r.q, r.qbuf.at[x], r.q_send.at[k], r.q_recv.at[k], along_x(k))
+    def q_piece(k, half):
+        at = pl.ds(0, rows) if half is None else pl.ds(half * (rows // 2), rows // 2)
+        return r.qbuf.at[lax.rem(x + k, NX), at]
+
+    gq = Gather4(q_piece, r.gq_send, r.gq_recv, 0, along_x(1), along_x(3))
 
     def weight_copies(k):
         to = lax.rem(x + k, NX)
         return [
-            remote(r.gu.at[to], r.gubuf.at[z, x], r.wx_send.at[k, 0], r.wx_recv.at[k, 0], along_x(k)),
+            remote(r.gustage.at[to], r.gubuf.at[z, x], r.wx_send.at[k, 0], r.wx_recv.at[k, 0], along_x(k)),
             remote(r.dn.at[to], r.dnbuf.at[z, x], r.wx_send.at[k, 1], r.wx_recv.at[k, 1], along_x(k)),
         ]
 
     def ow_copy(i):
         k, other = i // 2, i % 2
         to = along_y(k, other)
-        src = r.ow.at[:, pl.ds(pl.multiple_of(to[1] * cols, cols), cols)]
+        src = r.owstage.at[:, pl.ds(pl.multiple_of(to[1] * cols, cols), cols)]
         return remote(src, r.owbuf.at[tp], r.ow_send.at[i], r.ow_recv.at[i], to)
 
     for chunk in range(CHUNKS):
-        ring(None, 1, chunk, up).start()
-        ring(None, far + 1, chunk, down).start()
-    own_cols = pl.ds(pl.multiple_of(tp * cols, cols), cols)
-    local = [
-        pltpu.make_async_copy(r.lat, r.latbuf.at[0], r.local_sem.at[0]),
-        pltpu.make_async_copy(r.q, r.qbuf.at[x], r.local_sem.at[1]),
-        pltpu.make_async_copy(r.gu.at[x], r.gubuf.at[z, x], r.local_sem.at[2]),
-        pltpu.make_async_copy(r.dn.at[x], r.dnbuf.at[z, x], r.local_sem.at[3]),
-        pltpu.make_async_copy(r.ow.at[:, own_cols], r.owbuf.at[tp], r.local_sem.at[4]),
-        pltpu.make_async_copy(r.resid.at[:, own_cols], r.residbuf, r.local_sem.at[5]),
-    ]
-    for copy in local:
-        copy.start()
-    for k in range(1, NX):
-        q_copy(k).start()
-    for k in range(1, NX):
+        ring(0, 1, chunk, up).start()
+        ring(0, far + 1, chunk, down).start()
+    gq.start()
+
+    gain = column(r.ffn_gain[pl.ds(sp, 1), :])
+    gate, upward = r.gate[...].astype(F32) * gain, r.upward[...].astype(F32) * gain
+    for i in range(NX):
+        lo, mid_lo, hi = i * UNIT, i * UNIT + 128, (i + 1) * UNIT
+        tiles = [gate[:, lo:mid_lo], gate[:, mid_lo:hi], upward[:, mid_lo:hi], upward[:, lo:mid_lo]]
+        r.gustage[i] = jnp.concatenate(tiles, axis=1).astype(BF16)
+    local[3].start()
+    for k in (2, 1, 3):
         for copy in weight_copies(k):
             copy.start()
+    for h in range(2):
+        at = 2 * h * NOPE
+        r.wk[:, h * NOPE : (h + 1) * NOPE] = r.kv_weight[:, at : at + NOPE]
+        value_weight = r.kv_weight[:, at + NOPE : at + NOPE + VDIM].astype(F32)
+        r.wv[h * VDIM : (h + 1) * VDIM, :] = jnp.transpose(value_weight).astype(BF16)
+    local[0].wait()
+    gain = column(r.out_gain[...])
+
+    def scale_ow(j, carry):
+        at = pl.ds(pl.multiple_of(j * cols, cols), cols)
+        r.owstage[:, at] = (r.owstage[:, at].astype(F32) * gain).astype(BF16)
+        return carry
+
+    lax.fori_loop(0, NT, scale_ow, 0)
+    local[4].start()
     for i in range(1, NT):
         ow_copy(i).start()
 
@@ -207,17 +261,22 @@
     r.acc[...] = jnp.zeros(r.acc.shape, F32)
 
     def piece(slot, diagonal):
-        lat = r.latbuf[slot].reshape(rows, r.lat.shape[-1])
+        lat = r.latbuf[slot].reshape(rows, r.latbuf.shape[-1])
         wide = r.wk.shape[0]
-        compressed, key_rot = lat[:, :wide], lat[:, wide:]
+        compressed, both_rot = lat[:, :wide], lat[:, wide:]
+        lane = lax.broadcasted_iota(jnp.int32, both_rot.shape, 1)
         keys = wide_dot(compressed, r.wk[...]).astype(BF16)
         values = nt_dot(r.wv[...], compressed).astype(BF16)
         for h in range(2):
+            own_half = lane < ROPE if h == 0 else lane >= ROPE
+            key_rot = jnp.where(own_half, both_rot.astype(F32), 0.0).astype(BF16)
             key = jnp.concatenate([keys[:, h * NOPE : (h + 1) * NOPE], key_rot], axis=1)
             value = values[h * VDIM : (h + 1) * VDIM]
             for b in range(NX):
                 at = pl.ds(b * rows, rows)
-                scores = nt_dot(key, r.qbuf[b, h]) * factor
+                here = r.qbuf[b, :, h * NOPE : (h + 1) * NOPE]
+                turned_here = r.qbuf[b, :, 2 * NOPE :]
+                scores = nt_dot(key, jnp.concatenate([here, turned_here], axis=1)) * factor
                 if diagonal:
                     key_at = x * rows + lax.broadcasted_iota(jnp.int32, scores.shape, 0)
                     query_at = b * rows + lax.broadcasted_iota(jnp.int32, scores.shape, 1)
@@ -235,15 +294,9 @@
                 )
                 r.acc[h, :, at] = r.acc[h, :, at] * shrink + wide_dot(value, weights.astype(BF16))
 
-    for copy in local[:2]:
-        copy.wait()
-    for k in range(1, NX):
-        q_copy(k).wait_recv()
-    piece(0, True)
-
     def arrive(slot, forward_to, to):
         for chunk in range(CHUNKS):
-            ring(None, slot, chunk, to).wait_recv()
+            ring(0, slot, chunk, to).wait_recv()
             if forward_to is not None:
                 ring(slot, forward_to, chunk, to).start()
             pair(slot, chunk, core).start()
@@ -284,7 +337,7 @@
         for k in range(1, NX):
             for copy in weight_copies(k):
                 copy.wait_recv()
-        local[2].wait()
+        local[1].wait()
         local[3].wait()
         for way, part in in_hop(1):
             hop(1, way, part).start()
@@ -295,14 +348,27 @@
             if d < far and (way, part) in in_hop(d + 1):
                 hop(d + 1, way, part).start()
 
-    for d in range(1, far + 1):
+    def hop_latent(d):
         arrive(d, d + 1 if d < far else None, up)
         if d < far:
             arrive(far + d, far + d + 1 if d < far - 1 else None, down)
-        if d == far:
-            hop_first()
-        if d > 1:
-            lax.fori_loop(0, 2, both(d - 1), 0)
+
+    hop_latent(1)
+    gq.near(0)
+    gq.near(1)
+    hop_latent(2)
+    gq.far(0)
+    gq.far(1)
+    piece(0, True)
+    if far > 2:
+        lax.fori_loop(0, 2, both(1), 0)
+        hop_latent(3)
+    for d in range(2, far - 1):
+        lax.fori_loop(0, 2, both(d), 0)
+    hop_first()
+    if far > 3:
+        hop_latent(4)
+    lax.fori_loop(0, 2, both(far - 1), 0)
     use(far, z - far >= 0)
 
     for b in range(NX):
@@ -366,6 +432,7 @@
     swaps[1][0]().start()
     ga.near(1)
     swaps[2][0]().start()
+    hop_on(1)
     ga.far(0)
     swaps[3][0]().start()
     ga.far(1)
@@ -373,8 +440,7 @@
     for i in range(1, NT):
         ow_copy(i).wait_recv()
     local[4].wait()
-    local[5].wait()
-    hop_on(1)
+    local[2].wait()
     for out, come in swaps:
         come().wait_recv()
 
@@ -542,7 +608,6 @@
         r.out[:, at] = (s.total() + r.mid[x, own_rows, at].astype(F32)).astype(BF16)
 
     for k in range(1, NX):
-        q_copy(k).wait_send()
         o_copy(k).wait_send()
         s_copy(k).wait_send()
         for copy in weight_copies(k):
@@ -551,11 +616,12 @@
         ow_copy(i).wait_send()
     for slot in range(1, nz):
         for chunk in range(CHUNKS):
-            ring(None, slot, chunk, up).wait_send()
+            ring(0, slot, chunk, up).wait_send()
             pair(slot, chunk, core).wait_send()
     for d in range(1, far + 1):
         for way, part in in_hop(d):
             hop(d, way, part).wait_send()
+    gq.done()
     ga.done()
     for out, come in swaps:
         out().wait_send()
@@ -571,28 +637,26 @@
             s.done()
 
 
-def layer(lat, q, wk, wv, gu, dn, ow, resid):
+def layer(inputs, whole):
     nz = lax.axis_size("sp") // NX
-    rows, wide = lat.shape
-    dim = resid.shape[1]
+    vmem = pl.BlockSpec(memory_space=pltpu.VMEM)
+    anywhere = pl.BlockSpec(memory_space=pl.ANY)
+    rows, wide = inputs["latent"].shape
+    depth = inputs["gate"].shape[0]
+    n = inputs["dn"].shape[-1]
+    dim = inputs["resid"].shape[1]
     share = rows // NT
     cols = dim // NT
-    lat = lat.reshape(NC, CHUNKS, rows // NC // CHUNKS, wide)
-    vmem = pl.BlockSpec(memory_space=pltpu.VMEM)
-    anywhere = pl.BlockSpec(memory_space=pl.ANY)
-    inputs = {
-        "lat": (lat, vmem),
-        "q": (q, vmem),
-        "wk": (wk, vmem),
-        "wv": (wv, vmem),
-        "gu": (gu, anywhere),
-        "dn": (dn, anywhere),
-        "ow": (ow, anywhere),
-        "resid": (resid, anywhere),
-    }
+    lat = (NC, CHUNKS, rows // NC // CHUNKS, wide + 2 * ROPE)
+    gu, dn = (NX, depth, 2 * UNIT), (NX, UNIT, n)
+    heads = 2 * VDIM
     buffers = {
-        "latbuf": ((nz, *lat.shape), BF16),
-        "qbuf": ((NX, *q.shape), BF16),
+        "latbuf": ((nz, *lat), BF16),
+        "qbuf": ((NX, rows, 2 * (NOPE + ROPE)), BF16),
+        "wk": ((wide, 2 * NOPE), BF16),
+        "wv": ((heads, wide), BF16),
+        "gustage": (gu, BF16),
+        "owstage": ((heads, dim), BF16),
         "acc": ((2, VDIM, NX * rows), F32),
         "stat_m": ((2, 1, NX * rows), F32),
         "stat_l": ((2, 1, NX * rows), F32),
@@ -600,9 +664,9 @@
         "orecv": ((NX, 2 * VDIM, rows), BF16),
         "ssend": ((NX, 8, rows), F32),
         "srecv": ((NX, 8, rows), F32),
-        "gubuf": ((nz, *gu.shape), BF16),
-        "dnbuf": ((nz, *dn.shape), BF16),
-        "owbuf": ((NT, ow.shape[0], cols), BF16),
+        "gubuf": ((nz, *gu), BF16),
+        "dnbuf": ((nz, *dn), BF16),
+        "owbuf": ((NT, heads, cols), BF16),
         "residbuf": ((rows, cols), BF16),
         "att": ((rows, NT * 2 * VDIM), BF16),
         "mid": ((NX, rows, dim), BF16),
@@ -612,13 +676,13 @@
         "whole_in": ((10, 2, share, dim // 2), BF16),
     }
     semaphores = {
-        "local_sem": (6,),
+        "local_sem": (5,),
         "ring_send": (nz, CHUNKS),
         "ring_recv": (nz, CHUNKS),
         "pair_send": (nz, CHUNKS),
         "pair_recv": (nz, CHUNKS),
-        "q_send": (NX,),
-        "q_recv": (NX,),
+        "gq_send": (1, 4),
+        "gq_recv": (1, 4),
         "wx_send": (NX, 2),
         "wx_recv": (NX, 2),
         "ow_send": (NT,),
@@ -646,22 +710,14 @@
     return pl.pallas_call(
         functools.partial(layer_kernel, nz, names),
         out_shape=jax.ShapeDtypeStruct((share, dim), BF16),
-        in_specs=[spec for _, spec in inputs.values()],
+        in_specs=[anywhere if name in whole else vmem for name in inputs],
         out_specs=vmem,
         scratch_shapes=[pltpu.VMEM(*b) for b in buffers.values()]
         + [pltpu.SemaphoreType.DMA(s) for s in semaphores.values()],
         compiler_params=pltpu.CompilerParams(
             collective_id=0, has_side_effects=True, vmem_limit_bytes=62 * 1024 * 1024
         ),
-    )(*[array for array, _ in inputs.values()])
-
-
-def turned(values, cosine, sine):
-    half = values.shape[-1] // 2
-    first, second = values[..., :half], values[..., half:]
-    return jnp.concatenate(
-        [first * cosine - second * sine, first * sine + second * cosine], axis=-1
-    )
+    )(*inputs.values())
 
 
 def body(
@@ -679,50 +735,30 @@
     down_weight,
 ):
     rows = latent.shape[0]
-    sp = lax.axis_index("sp")
-    heads_here = queries.shape[1] // (NOPE + ROPE)
-    places = (sp * rows + jnp.arange(rows, dtype=jnp.int32)).astype(F32)
     half = ROPE // 2
-    inverse = THETA ** (-jnp.arange(half, dtype=F32) / half)
-    angle = places[:, None] * inverse
-    cosine, sine = jnp.cos(angle), jnp.sin(angle)
-    pad = jnp.zeros((rows, NOPE - ROPE), BF16)
-    key_rot = turned(rope_key.astype(F32), cosine, sine).astype(BF16)
-    normed = norm_rows(latent, lat_gain).astype(BF16)
-    lat = jnp.concatenate([normed, key_rot, pad], axis=1)
-    query = queries.reshape(rows, heads_here, NOPE + ROPE)
-    query_rot = turned(
-        query[:, :, NOPE:].astype(F32), cosine[:, None], sine[:, None]
-    ).astype(BF16)
-    full = jnp.concatenate(
-        [query[:, :, :NOPE], query_rot, jnp.broadcast_to(pad[:, None], (rows, heads_here, NOPE - ROPE))],
-        axis=2,
-    )
-    full = jnp.transpose(full, (1, 0, 2))
-    weight = kv_weight.reshape(kv_weight.shape[0], heads_here, NOPE + VDIM)
-    wk = weight[:, :, :NOPE].reshape(-1, heads_here * NOPE)
-    wv = jnp.transpose(weight[:, :, NOPE:].reshape(-1, heads_here * VDIM))
-    depth = gate_weight.shape[0]
-    gain = lax.dynamic_slice_in_dim(ffn_gain, sp * depth, depth)[:, None]
-    gate = (gate_weight.astype(F32) * gain).astype(BF16)
-    upward = (up_weight.astype(F32) * gain).astype(BF16)
-    gu = jnp.stack(
-        [
-            jnp.concatenate(
-                [
-                    gate[:, i * UNIT : i * UNIT + 128],
-                    gate[:, i * UNIT + 128 : (i + 1) * UNIT],
-                    upward[:, i * UNIT + 128 : (i + 1) * UNIT],
-                    upward[:, i * UNIT : i * UNIT + 128],
-                ],
-                axis=1,
-            )
-            for i in range(NX)
-        ]
-    )
-    dn = down_weight.reshape(NX, UNIT, down_weight.shape[1])
-    ow = (out_weight.astype(F32) * out_gain[:, None]).astype(BF16)
-    return layer(lat, full, wk, wv, gu, dn, ow, resid)
+    frequency = THETA ** (-np.arange(half) / half)
+
+    def turns(places):
+        angle = places[:, None] * frequency
+        return jnp.asarray(np.concatenate([np.cos(angle), np.sin(angle)], axis=1), F32)
+
+    inputs = {
+        "latent": latent,
+        "rope_key": rope_key,
+        "queries": queries,
+        "lat_gain": lat_gain[None, :],
+        "kv_weight": kv_weight,
+        "gate": gate_weight,
+        "upward": up_weight,
+        "ffn_gain": ffn_gain.reshape(-1, gate_weight.shape[0]),
+        "out_gain": out_gain[None, :],
+        "first_turn": turns(np.arange(lax.axis_size("sp")) * rows),
+        "row_turn": turns(np.arange(rows)),
+        "dn": down_weight.reshape(NX, UNIT, down_weight.shape[1]),
+        "ow": out_weight,
+        "resid": resid,
+    }
+    return layer(inputs, ("dn", "ow", "resid"))
 
 
 def solution(mesh):

time: 159 us -> 143 us (0.90)
  other arithmetic: 7.11 us -> 0 us
  Pallas kernels: 144 us -> 139 us
  local copies, waits for them, and re-layouts: 6.78 us -> 3.16 us
    pallas_call x1, Pallas kernels: 144 us -> 139 us  [layer(): pl.pallas_call(functools.partial(layer_kernel, nz, names), out_shape=jax....]
    convert_element_type x6 -> x0, other arithmetic: 2.96 us -> none  [the longest x1 1.92 us: body(): ow = (out_weight.astype(F32) * out_gain[:, None]).astype(BF16)]
    unnamed x20 -> x2, local copies, waits for them, and re-layouts: 4.64 us -> 3.16 us
where the time goes in v3:
time: 143 us; the launch traced here: 142 us
  Pallas kernels  139 us (97%)
  local copies, waits for them, and re-layouts  3.16 us (2%)
    pallas_call x1, Pallas kernels, layer(): pl.pallas_call(functools.partial(layer_kernel, nz, names), out_shape=jax....  139 us
    unnamed x2, local copies, waits for them, and re-layouts  3.16 us

profile of v3, /device:TPU:1, one launch (start us, length us, event | category | flops | bytes accessed | tf_op | source)
XLA Modules:
  0.0 142.1 jit_solution(358144727246575478)
XLA Ops:
  0.0 1.5 %copy.15.values_1_ = bf16[256,64]{1,0:T(8,128)(2,1)} copy(bf16[256,64]{0,1:T(8,128)(2,1)} %param.17) | data formatting | bytes 65536 | tf_op args[3]
  1.5 138.9 %shard_map.136 = bf16[32,4096]{1,0:T(8,128)(2,1)} custom-call(bf16[256,512]{1,0:T(8,128)(2,1)} %values_0_.1, bf16[256,64]{1,0:T(8,128)(2,1)} %copy.15.values_1_, bf16[256,384]{1,0:T(8,128)(2,1)} %values_2_.1, f32[1,512]{1,0:T(1,128)} %bitcast.6, bf16[512,512]{1,0:T(8,128)(2,1)} %values_4_.1, bf16[128,768]{1,0:T(8,128)(2,1)} %values_5_.1, ...), custom_call_target="tpu_custom_call" | custom-call | tf_op jit(solution)/shard_map/pallas_call | solution.py:710
  140.4 1.7 %copy.17 = bf16[32,4096]{1,0:T(8,128)(2,1)} copy(bf16[32,4096]{1,0:T(8,128)(2,1)} %shard_map.136) | data formatting | bytes 524288

commit v4 on v3

--- a/solution.py
+++ b/solution.py
@@ -192,7 +192,8 @@
     one = NOPE + ROPE
     parts = [query[:, h * one : h * one + NOPE] for h in range(2)]
     parts += [turned(query[:, h * one + NOPE : (h + 1) * one], cosine, sine) for h in range(2)]
-    r.qbuf[x] = jnp.concatenate(parts, axis=1).astype(BF16)
+    own_rows_at = pl.ds(pl.multiple_of(x * rows, rows), rows)
+    r.qbuf[:, own_rows_at] = jnp.transpose(jnp.concatenate(parts, axis=1)).astype(BF16)
     pl.semaphore_wait(barrier, len(peers))
 
     def ring(src_slot, dst_slot, chunk, to):
@@ -205,8 +206,9 @@
         return remote(ref, ref, r.pair_send.at[slot, chunk], r.pair_recv.at[slot, chunk], partner)
 
     def q_piece(k, half):
-        at = pl.ds(0, rows) if half is None else pl.ds(half * (rows // 2), rows // 2)
-        return r.qbuf.at[lax.rem(x + k, NX), at]
+        channels = r.qbuf.shape[0]
+        at = pl.ds(0, channels) if half is None else pl.ds(half * (channels // 2), channels // 2)
+        return r.qbuf.at[at, pl.ds(pl.multiple_of(lax.rem(x + k, NX) * rows, rows), rows)]
 
     gq = Gather4(q_piece, r.gq_send, r.gq_recv, 0, along_x(1), along_x(3))
 
@@ -235,7 +237,7 @@
         tiles = [gate[:, lo:mid_lo], gate[:, mid_lo:hi], upward[:, mid_lo:hi], upward[:, lo:mid_lo]]
         r.gustage[i] = jnp.concatenate(tiles, axis=1).astype(BF16)
     local[3].start()
-    for k in (2, 1, 3):
+    for k in (1, 3):
         for copy in weight_copies(k):
             copy.start()
     for h in range(2):
@@ -271,15 +273,17 @@
             own_half = lane < ROPE if h == 0 else lane >= ROPE
             key_rot = jnp.where(own_half, both_rot.astype(F32), 0.0).astype(BF16)
             key = jnp.concatenate([keys[:, h * NOPE : (h + 1) * NOPE], key_rot], axis=1)
-            value = values[h * VDIM : (h + 1) * VDIM]
-            for b in range(NX):
-                at = pl.ds(b * rows, rows)
-                here = r.qbuf[b, :, h * NOPE : (h + 1) * NOPE]
-                turned_here = r.qbuf[b, :, 2 * NOPE :]
-                scores = nt_dot(key, jnp.concatenate([here, turned_here], axis=1)) * factor
+            query = jnp.concatenate(
+                [r.qbuf[h * NOPE : (h + 1) * NOPE], r.qbuf[2 * NOPE :]], axis=0
+            )
+            r.scores[h] = wide_dot(key, query)
+        for h in range(2):
+            for b in range(NX * rows // 128):
+                at = pl.ds(b * 128, 128)
+                scores = r.scores[h, :, at] * factor
                 if diagonal:
                     key_at = x * rows + lax.broadcasted_iota(jnp.int32, scores.shape, 0)
-                    query_at = b * rows + lax.broadcasted_iota(jnp.int32, scores.shape, 1)
+                    query_at = b * 128 + lax.broadcasted_iota(jnp.int32, scores.shape, 1)
                     allowed = key_at <= query_at
                     scores = jnp.where(allowed, scores, LOWEST)
                 old = r.stat_m[h, :, at]
@@ -289,10 +293,13 @@
                     weights = jnp.where(allowed, weights, 0.0)
                 shrink = jnp.exp2(old - new)
                 r.stat_m[h, :, at] = new
+                r.stat_a[h, :, at] = shrink
                 r.stat_l[h, :, at] = r.stat_l[h, :, at] * shrink + jnp.sum(
                     weights, axis=0, keepdims=True
                 )
-                r.acc[h, :, at] = r.acc[h, :, at] * shrink + wide_dot(value, weights.astype(BF16))
+                r.weights[h, :, at] = weights.astype(BF16)
+            value = values[h * VDIM : (h + 1) * VDIM]
+            r.acc[h] = r.acc[h] * r.stat_a[h] + wide_dot(value, r.weights[h])
 
     def arrive(slot, forward_to, to):
         for chunk in range(CHUNKS):
@@ -342,8 +349,10 @@
         for way, part in in_hop(1):
             hop(1, way, part).start()
 
-    def hop_on(d):
+    def hop_on(d, only=None):
         for way, part in in_hop(d):
+            if only is not None and part != only:
+                continue
             hop_in(d, way, part).wait_recv()
             if d < far and (way, part) in in_hop(d + 1):
                 hop(d + 1, way, part).start()
@@ -356,6 +365,8 @@
     hop_latent(1)
     gq.near(0)
     gq.near(1)
+    for copy in weight_copies(2):
+        copy.start()
     hop_latent(2)
     gq.far(0)
     gq.far(1)
@@ -416,6 +427,7 @@
 
         return ref
 
+    hop_on(1, 0)
     ga = Gather4(att_piece(core), r.ga_send, r.ga_recv, 0, along_y(1), along_y(3))
 
     def swap(piece, send, recv, index):
@@ -432,7 +444,7 @@
     swaps[1][0]().start()
     ga.near(1)
     swaps[2][0]().start()
-    hop_on(1)
+    hop_on(1, 1)
     ga.far(0)
     swaps[3][0]().start()
     ga.far(1)
@@ -484,16 +496,17 @@
             g.near(way)
             second_rings[1 + way][i][0].start()
             s[1 + way][0]().start()
+    hop_on(2, 0)
     for way in range(2):
         for g, s in second_rings[0]:
             g.near(way)
             s[1 + way][0]().start()
+    hop_on(2, 1)
     for i, (g, s) in enumerate(first_rings):
         for half in range(2):
             g.far(half)
             s[3 + half][0]().start()
         second_rings[3][i][0].start()
-    hop_on(2)
     for j in range(1, 4):
         for way in range(2):
             for g, s in second_rings[j]:
@@ -503,8 +516,10 @@
             for g, s in second_rings[j - 1]:
                 g.far(half)
                 s[3 + half][0]().start()
+        if j == 1 and far > 3:
+            hop_on(3, 0)
         if j == 2 and far > 3:
-            hop_on(3)
+            hop_on(3, 1)
     for half in range(2):
         for g, s in second_rings[3]:
             g.far(half)
@@ -519,10 +534,11 @@
             if j > 0 or i < 2:
                 come().wait_recv()
 
-    def mixer(b, carry):
+    def mixer(j):
+        b = lax.rem(x + ahead(j), NX)
         squares = jnp.zeros((rows, 128), F32)
-        for j in range(r.mid.shape[2] // 128):
-            v = r.mid[b, :, j * 128 : (j + 1) * 128].astype(F32)
+        for i in range(r.mid.shape[2] // 128):
+            v = r.mid[b, :, i * 128 : (i + 1) * 128].astype(F32)
             squares = squares + v * v
         mean = jnp.sum(squares, axis=1, keepdims=True) / r.mid.shape[2]
         row_scale = lax.rsqrt(mean + EPSILON)
@@ -538,22 +554,21 @@
             terms = wide_dot(hidden, w).astype(BF16).reshape(NY, NC, share, NX * n)
             for c in range(NC):
                 r.part[c, b, :, :, zz * NX * n : (zz + 1) * NX * n] = terms[:, c]
-        core_copy(b).start()
-        return carry
-
-    def core_copy(b):
-        return remote(r.part.at[1 - core, b], r.pairbuf.at[b], r.pc_send.at[b], r.pc_recv.at[b], partner)
-
-    lax.fori_loop(0, NX, mixer, 0)
-
-    def core_sum(b, carry):
-        core_copy(b).wait_recv()
+        core_copy(j).start()
+
+    def ahead(j):
+        return jnp.where(j == 0, 2, jnp.where(j == 1, 1, jnp.where(j == 2, 3, 0)))
+
+    def core_copy(j):
+        b = lax.rem(x + ahead(j), NX)
+        return remote(r.part.at[1 - core, b], r.pairbuf.at[b], r.pc_send.at[j], r.pc_recv.at[j], partner)
+
+    def core_sum(j):
+        b = lax.rem(x + ahead(j), NX)
+        core_copy(j).wait_recv()
         for i in range(NY):
             ref = r.part.at[core, b, i]
             ref[...] = (ref[...].astype(F32) + r.pairbuf[b, i].astype(F32)).astype(BF16)
-        return carry
-
-    lax.fori_loop(0, NX, core_sum, 0)
 
     depth = r.part.shape[-1] // 2
 
@@ -581,22 +596,49 @@
             minus,
         )
 
-    order = (1, 3, 2, 0)
-    steps = [
-        [scatter(i, 1, x + k, y, 0), scatter(4 + i, 0, x, y + k, 1)] for i, k in enumerate(order)
-    ]
+    def first_along_y(j):
+        return scatter(j, 1, x + ahead(j), y, 0)
+
+    def first_along_x(j):
+        return scatter(4 + j, 0, x, y + ahead(j), 1)
+
+    def stage(j, carry):
+        @pl.when(j < NX)
+        def _():
+            mixer(j)
+
+        @pl.when(j >= 1)
+        def _():
+            core_sum(j - 1)
+            first_along_y(j - 1).start()
+
+        @pl.when(j == 1)
+        def _():
+            for i in range(NY):
+                first_along_x(i).start()
+
+        @pl.when(j >= 2)
+        def _():
+            first_along_y(j - 2).near(0)
+            first_along_y(j - 2).near(1)
+
+        @pl.when(j == NX - 1)
+        def _():
+            for i in range(NY):
+                first_along_x(i).near(0)
+                first_along_x(i).near(1)
+
+        return carry
+
+    lax.fori_loop(0, NX + 1, stage, 0)
+    steps = [[first_along_y(j), first_along_x(j)] for j in range(NX)]
     ends = [scatter(8, 0, x, y, 0), scatter(9, 1, x, y, 1)]
-    for both_of in steps:
-        for s in both_of:
-            s.start()
-    for both_of in steps:
-        for s in both_of:
-            s.near(0)
-            s.near(1)
+    first_along_y(NX - 1).near(0)
+    first_along_y(NX - 1).near(1)
     for j, both_of in enumerate(steps):
         for s in both_of:
             s.finish()
-        if j == 2:
+        if j == 0:
             for s in ends:
                 s.start()
     for s in ends:
@@ -630,8 +672,8 @@
         for j, (out, come) in enumerate(s):
             if j > 0 or i < 2:
                 out().wait_send()
-    for b in range(NX):
-        core_copy(b).wait_send()
+    for j in range(NX):
+        core_copy(j).wait_send()
     for both_of in [*steps, ends]:
         for s in both_of:
             s.done()
@@ -652,7 +694,10 @@
     heads = 2 * VDIM
     buffers = {
         "latbuf": ((nz, *lat), BF16),
-        "qbuf": ((NX, rows, 2 * (NOPE + ROPE)), BF16),
+        "qbuf": ((2 * (NOPE + ROPE), NX * rows), BF16),
+        "scores": ((2, rows, NX * rows), F32),
+        "weights": ((2, rows, NX * rows), BF16),
+        "stat_a": ((2, 1, NX * rows), F32),
         "wk": ((wide, 2 * NOPE), BF16),
         "wv": ((heads, wide), BF16),
         "gustage": (gu, BF16),

time: 143 us -> 122 us (0.85)
  Pallas kernels: 139 us -> 119 us
    pallas_call x1, Pallas kernels: 139 us -> 119 us  [layer(): pl.pallas_call(functools.partial(layer_kernel, nz, names), out_shape=jax....]
where the time goes in v4:
time: 122 us
  Pallas kernels  119 us (98%)
  local copies, waits for them, and re-layouts  3.16 us (3%)
    pallas_call x1, Pallas kernels, layer(): pl.pallas_call(functools.partial(layer_kernel, nz, names), out_shape=jax....  119 us
    unnamed x2, local copies, waits for them, and re-layouts  3.16 us

profile of v4, /device:TPU:1, one launch (start us, length us, event | category | flops | bytes accessed | tf_op | source)
XLA Modules:
  0.0 122.3 jit_solution(13418936265861094312)
XLA Ops:
  0.0 1.5 %copy.15.values_1_ = bf16[256,64]{1,0:T(8,128)(2,1)} copy(bf16[256,64]{0,1:T(8,128)(2,1)} %param.17) | data formatting | bytes 65536 | tf_op args[3]
  1.5 119.1 %shard_map.136 = bf16[32,4096]{1,0:T(8,128)(2,1)} custom-call(bf16[256,512]{1,0:T(8,128)(2,1)} %values_0_.1, bf16[256,64]{1,0:T(8,128)(2,1)} %copy.15.values_1_, bf16[256,384]{1,0:T(8,128)(2,1)} %values_2_.1, f32[1,512]{1,0:T(1,128)} %bitcast.6, bf16[512,512]{1,0:T(8,128)(2,1)} %values_4_.1, bf16[128,768]{1,0:T(8,128)(2,1)} %values_5_.1, ...), custom_call_target="tpu_custom_call" | custom-call | tf_op jit(solution)/shard_map/pallas_call | solution.py:755
  120.6 1.7 %copy.17 = bf16[32,4096]{1,0:T(8,128)(2,1)} copy(bf16[32,4096]{1,0:T(8,128)(2,1)} %shard_map.136) | data formatting | bytes 524288

commit v5 on v4

--- a/solution.py
+++ b/solution.py
@@ -16,7 +16,8 @@
 NY = 4
 NC = 2
 NT = NY * NC
-CHUNKS = 2
+CHUNKS = 4
+EARLY = 1
 UNIT = 192
 
 EPSILON = 1e-06
@@ -169,11 +170,18 @@
         pl.semaphore_signal(barrier, inc=1, device_id=peer, device_id_type=MESH)
 
     own_cols = pl.ds(pl.multiple_of(tp * cols, cols), cols)
+
+    def place(t, at_z):
+        return lax.rem(t - at_z + far + nz, nz)
+
+    def channels(t):
+        return pl.ds(pl.multiple_of(place(t, z) * cols, cols), cols)
+
     local = [
         pltpu.make_async_copy(r.ow, r.owstage, r.local_sem.at[0]),
         pltpu.make_async_copy(r.dn.at[x], r.dnbuf.at[z, x], r.local_sem.at[1]),
         pltpu.make_async_copy(r.resid.at[:, own_cols], r.residbuf, r.local_sem.at[2]),
-        pltpu.make_async_copy(r.gustage.at[x], r.gubuf.at[z, x], r.local_sem.at[3]),
+        pltpu.make_async_copy(r.gustage.at[x], r.gubuf.at[far, x], r.local_sem.at[3]),
         pltpu.make_async_copy(r.owstage.at[:, own_cols], r.owbuf.at[tp], r.local_sem.at[4]),
     ]
     for copy in local[:3]:
@@ -185,7 +193,7 @@
     step_cos, step_sin = step[:, :half], step[:, half:]
     cosine = base_cos * step_cos - base_sin * step_sin
     sine = base_sin * step_cos + base_cos * step_sin
-    key_rot = turned(r.rope_key[...].astype(F32), cosine, sine)
+    key_rot = turned(jnp.transpose(r.rope_key[...].astype(F32)), cosine, sine)
     lat = jnp.concatenate([norm_rows(r.latent[...], r.lat_gain[...]), key_rot, key_rot], axis=1)
     r.latbuf[0] = lat.astype(BF16).reshape(r.latbuf.shape[1:])
     query = r.queries[...].astype(F32)
@@ -215,7 +223,7 @@
     def weight_copies(k):
         to = lax.rem(x + k, NX)
         return [
-            remote(r.gustage.at[to], r.gubuf.at[z, x], r.wx_send.at[k, 0], r.wx_recv.at[k, 0], along_x(k)),
+            remote(r.gustage.at[to], r.gubuf.at[far, x], r.wx_send.at[k, 0], r.wx_recv.at[k, 0], along_x(k)),
             remote(r.dn.at[to], r.dnbuf.at[z, x], r.wx_send.at[k, 1], r.wx_recv.at[k, 1], along_x(k)),
         ]
 
@@ -262,28 +270,38 @@
     r.stat_l[...] = jnp.zeros(r.stat_l.shape, F32)
     r.acc[...] = jnp.zeros(r.acc.shape, F32)
 
-    def piece(slot, diagonal):
+    def keys_of(slot):
         lat = r.latbuf[slot].reshape(rows, r.latbuf.shape[-1])
         wide = r.wk.shape[0]
         compressed, both_rot = lat[:, :wide], lat[:, wide:]
         lane = lax.broadcasted_iota(jnp.int32, both_rot.shape, 1)
         keys = wide_dot(compressed, r.wk[...]).astype(BF16)
         values = nt_dot(r.wv[...], compressed).astype(BF16)
+        out = []
         for h in range(2):
             own_half = lane < ROPE if h == 0 else lane >= ROPE
             key_rot = jnp.where(own_half, both_rot.astype(F32), 0.0).astype(BF16)
             key = jnp.concatenate([keys[:, h * NOPE : (h + 1) * NOPE], key_rot], axis=1)
+            out.append((key, values[h * VDIM : (h + 1) * VDIM]))
+        return out
+
+    def attend(heads_here, first, count, diagonal):
+        for h, (key, _) in enumerate(heads_here):
+            at = pl.ds(first, count)
             query = jnp.concatenate(
-                [r.qbuf[h * NOPE : (h + 1) * NOPE], r.qbuf[2 * NOPE :]], axis=0
+                [r.qbuf[h * NOPE : (h + 1) * NOPE, at], r.qbuf[2 * NOPE :, at]], axis=0
             )
-            r.scores[h] = wide_dot(key, query)
-        for h in range(2):
-            for b in range(NX * rows // 128):
-                at = pl.ds(b * 128, 128)
-                scores = r.scores[h, :, at] * factor
+            r.scores[h, :, :count] = wide_dot(key, query)
+        for h, (_, value) in enumerate(heads_here):
+            for b in range(count // 128):
+                here = pl.ds(b * 128, 128)
+                at = pl.ds(first + b * 128, 128)
+                if not isinstance(first, int):
+                    at = pl.ds(pl.multiple_of(first + b * 128, 128), 128)
+                scores = r.scores[h, :, here] * factor
                 if diagonal:
                     key_at = x * rows + lax.broadcasted_iota(jnp.int32, scores.shape, 0)
-                    query_at = b * 128 + lax.broadcasted_iota(jnp.int32, scores.shape, 1)
+                    query_at = first + b * 128 + lax.broadcasted_iota(jnp.int32, scores.shape, 1)
                     allowed = key_at <= query_at
                     scores = jnp.where(allowed, scores, LOWEST)
                 old = r.stat_m[h, :, at]
@@ -293,13 +311,21 @@
                     weights = jnp.where(allowed, weights, 0.0)
                 shrink = jnp.exp2(old - new)
                 r.stat_m[h, :, at] = new
-                r.stat_a[h, :, at] = shrink
+                r.stat_a[h, :, here] = shrink
                 r.stat_l[h, :, at] = r.stat_l[h, :, at] * shrink + jnp.sum(
                     weights, axis=0, keepdims=True
                 )
-                r.weights[h, :, at] = weights.astype(BF16)
-            value = values[h * VDIM : (h + 1) * VDIM]
-            r.acc[h] = r.acc[h] * r.stat_a[h] + wide_dot(value, r.weights[h])
+                r.weights[h, :, here] = weights.astype(BF16)
+            at = pl.ds(first, count)
+            r.acc[h, :, at] = r.acc[h, :, at] * r.stat_a[h, :, :count] + wide_dot(
+                value, r.weights[h, :, :count]
+            )
+
+    def piece(slot):
+        attend(keys_of(slot), 0, NX * rows, False)
+
+    def diagonal_part(heads_here, k):
+        attend(heads_here, pl.multiple_of(lax.rem(x + k, NX) * rows, rows), rows, True)
 
     def arrive(slot, forward_to, to):
         for chunk in range(CHUNKS):
@@ -314,7 +340,7 @@
 
         @pl.when(needed)
         def _():
-            piece(slot, False)
+            piece(slot)
 
     def both(d):
         def one(i, carry):
@@ -325,35 +351,58 @@
 
         return one
 
+    def hop_refs(of, way, part, z_from, z_to):
+        if part == 1:
+            return r.dnbuf.at[of], r.dnbuf.at[of]
+        return r.gubuf.at[place(of, z_from)], r.gubuf.at[place(of, z_to)]
+
     def hop(d, way, part):
         of = lax.rem(z - (d - 1) + nz, nz) if way == 0 else lax.rem(z + d - 1, nz)
-        ref = (r.gubuf if part == 0 else r.dnbuf).at[of]
         to = up if way == 0 else down
-        return remote(ref, ref, r.hop_send.at[d, way, part], r.hop_recv.at[d, way, part], to)
+        src, dst = hop_refs(of, way, part, z, to[0] // NX)
+        return remote(src, dst, r.hop_send.at[d, way, part], r.hop_recv.at[d, way, part], to)
 
     def hop_in(d, way, part):
         of = lax.rem(z - d + nz, nz) if way == 0 else lax.rem(z + d, nz)
-        ref = (r.gubuf if part == 0 else r.dnbuf).at[of]
         to = up if way == 0 else down
-        return remote(ref, ref, r.hop_send.at[d, way, part], r.hop_recv.at[d, way, part], to)
+        src, dst = hop_refs(of, way, part, z, z)
+        return remote(src, dst, r.hop_send.at[d, way, part], r.hop_recv.at[d, way, part], to)
 
     def in_hop(d):
         return [(way, part) for part in range(2) for way in range(2) if d < far or way == part]
 
-    def hop_first():
-        for k in range(1, NX):
-            for copy in weight_copies(k):
+    def first_hop(k, way, part):
+        to = up if way == 0 else down
+        src, dst = hop_refs(z, way, part, z, to[0] // NX)
+        block = lax.rem(x + k, NX)
+        send, recv = r.first_send.at[k, way, part], r.first_recv.at[k, way, part]
+        return remote(src.at[block], dst.at[block], send, recv, to)
+
+    def first_in(k, way, part):
+        to = up if way == 0 else down
+        of = lax.rem(z + nz - 1, nz) if way == 0 else lax.rem(z + 1, nz)
+        ref = hop_refs(of, way, part, z, z)[0].at[lax.rem(x + k, NX)]
+        return remote(ref, ref, r.first_send.at[k, way, part], r.first_recv.at[k, way, part], to)
+
+    def start_first(k):
+        if k == 0:
+            local[1].wait()
+            local[3].wait()
+        else:
+            for copy in weight_copies(NX - k):
                 copy.wait_recv()
-        local[1].wait()
-        local[3].wait()
         for way, part in in_hop(1):
-            hop(1, way, part).start()
+            first_hop(k, way, part).start()
 
     def hop_on(d, only=None):
         for way, part in in_hop(d):
             if only is not None and part != only:
                 continue
-            hop_in(d, way, part).wait_recv()
+            if d == 1:
+                for k in range(NX):
+                    first_in(k, way, part).wait_recv()
+            else:
+                hop_in(d, way, part).wait_recv()
             if d < far and (way, part) in in_hop(d + 1):
                 hop(d + 1, way, part).start()
 
@@ -362,21 +411,28 @@
         if d < far:
             arrive(far + d, far + d + 1 if d < far - 1 else None, down)
 
+    own_keys = keys_of(0)
+    diagonal_part(own_keys, 0)
     hop_latent(1)
     gq.near(0)
     gq.near(1)
     for copy in weight_copies(2):
         copy.start()
+    diagonal_part(own_keys, 3)
+    diagonal_part(own_keys, 1)
     hop_latent(2)
     gq.far(0)
     gq.far(1)
-    piece(0, True)
+    diagonal_part(own_keys, 2)
     if far > 2:
         lax.fori_loop(0, 2, both(1), 0)
         hop_latent(3)
+    start_first(0)
+    start_first(1)
+    start_first(3)
     for d in range(2, far - 1):
         lax.fori_loop(0, 2, both(d), 0)
-    hop_first()
+    start_first(2)
     if far > 3:
         hop_latent(4)
     lax.fori_loop(0, 2, both(far - 1), 0)
@@ -391,23 +447,47 @@
             r.ssend[b, h : h + 1] = r.stat_m[h, :, at]
             r.ssend[b, 2 + h : 3 + h] = total
 
-    def o_copy(k):
+    def o_copy(k, h):
         to = lax.rem(x + k, NX)
-        return remote(r.osend.at[to], r.orecv.at[k], r.o_send.at[k], r.o_recv.at[k], along_x(k))
+        head = pl.ds(h * VDIM, VDIM)
+        return remote(
+            r.osend.at[to, head], r.orecv.at[k, head], r.o_send.at[k, h], r.o_recv.at[k, h], along_x(k)
+        )
 
     def s_copy(k):
         to = lax.rem(x + k, NX)
         return remote(r.ssend.at[to], r.srecv.at[k], r.s_send.at[k], r.s_recv.at[k], along_x(k))
 
-    for k in range(1, NX):
+    for k in (2, 1, 3):
         s_copy(k).start()
-        o_copy(k).start()
+    for h in range(2):
+        for k in (2, 1, 3):
+            o_copy(k, h).start()
     for k in range(1, NX):
         s_copy(k).wait_recv()
-        o_copy(k).wait_recv()
     width = 2 * VDIM
     stats = [r.ssend[x]] + [r.srecv[k] for k in range(1, NX)]
+
+    def swap(piece, send, recv, index):
+        k, half = ((0, None), (3, None), (1, None), (2, 0), (2, 1))[index]
+        mine, theirs = piece(core)(k, half), piece(1 - core)(k, half)
+        out = functools.partial(remote, mine, mine, send.at[index], recv.at[index], partner)
+        come = functools.partial(remote, theirs, theirs, send.at[index], recv.at[index], partner)
+        return out, come
+
+    def att_piece(h, own_core):
+        def ref(k, half):
+            of = lax.rem(y + k, NY) * NC + own_core
+            where = pl.ds(pl.multiple_of(of * width + h * VDIM, VDIM), VDIM)
+            at = pl.ds(0, rows) if half is None else pl.ds(half * (rows // 2), rows // 2)
+            return r.att.at[at, where]
+
+        return ref
+
+    heads = []
     for h in range(2):
+        for k in range(1, NX):
+            o_copy(k, h).wait_recv()
         outs = [r.osend[x, h * VDIM : (h + 1) * VDIM]] + [
             r.orecv[k, h * VDIM : (h + 1) * VDIM] for k in range(1, NX)
         ]
@@ -417,56 +497,71 @@
         mixed = sum(o.astype(F32) * (w * inverse) for o, w in zip(outs, shares))
         at = pl.ds(pl.multiple_of(tp * width + h * VDIM, VDIM), VDIM)
         r.att[:, at] = jnp.transpose(mixed).astype(BF16)
-
-    def att_piece(own_core):
-        def ref(k, half):
-            of = lax.rem(y + k, NY) * NC + own_core
-            where = pl.ds(pl.multiple_of(of * width, width), width)
-            at = pl.ds(0, rows) if half is None else pl.ds(half * (rows // 2), rows // 2)
-            return r.att.at[at, where]
-
-        return ref
-
+        piece_of = functools.partial(att_piece, h)
+        g = Gather4(piece_of(core), r.ga_send, r.ga_recv, h, along_y(1), along_y(3))
+        swaps = [swap(piece_of, r.sa_send.at[h], r.sa_recv.at[h], i) for i in range(5)]
+        g.start()
+        swaps[0][0]().start()
+        heads.append((g, swaps))
     hop_on(1, 0)
-    ga = Gather4(att_piece(core), r.ga_send, r.ga_recv, 0, along_y(1), along_y(3))
-
-    def swap(piece, send, recv, index):
-        k, half = ((0, None), (3, None), (1, None), (2, 0), (2, 1))[index]
-        mine, theirs = piece(core)(k, half), piece(1 - core)(k, half)
-        out = functools.partial(remote, mine, mine, send.at[index], recv.at[index], partner)
-        come = functools.partial(remote, theirs, theirs, send.at[index], recv.at[index], partner)
-        return out, come
-
-    swaps = [swap(att_piece, r.sa_send.at[0], r.sa_recv.at[0], i) for i in range(5)]
-    ga.start()
-    swaps[0][0]().start()
-    ga.near(0)
-    swaps[1][0]().start()
-    ga.near(1)
-    swaps[2][0]().start()
+    for way in range(2):
+        for g, swaps in heads:
+            g.near(way)
+            swaps[1 + way][0]().start()
     hop_on(1, 1)
-    ga.far(0)
-    swaps[3][0]().start()
-    ga.far(1)
-    swaps[4][0]().start()
+    for half in range(2):
+        for g, swaps in heads:
+            g.far(half)
+            swaps[3 + half][0]().start()
     for i in range(1, NT):
         ow_copy(i).wait_recv()
     local[4].wait()
     local[2].wait()
-    for out, come in swaps:
-        come().wait_recv()
+    for g, swaps in heads:
+        for out, come in swaps:
+            come().wait_recv()
 
     att = r.att[...]
     att_wide = att.astype(F32)
     scale = lax.rsqrt(jnp.mean(att_wide * att_wide, axis=1, keepdims=True) + EPSILON)
     attn_sum = wide_dot(att, r.owbuf[...].reshape(att.shape[1], cols)) * scale
-    r.mid[x, :, own_cols] = (r.residbuf[...].astype(F32) + attn_sum).astype(BF16)
+    middle = (r.residbuf[...].astype(F32) + attn_sum).astype(BF16)
+    r.mid[x, :, channels(tp)] = middle
+
+    def sq_copy(i):
+        ref = r.sq_part.at[tp]
+        return remote(ref, ref, r.sq_send.at[i], r.sq_recv.at[i], along_y(i // 2, i % 2))
+
+    def sx_copy(k):
+        ref = r.sq_row.at[x]
+        return remote(ref, ref, r.sx_send.at[k], r.sx_recv.at[k], along_x(k))
+
+    def squares_start():
+        wide = middle.astype(F32)
+        squares = jnp.sum(wide * wide, axis=1, keepdims=True)
+        r.sq_part[tp] = jnp.transpose(jnp.broadcast_to(squares, (rows, 128)))[:8]
+        for i in range(1, NT):
+            sq_copy(i).start()
+
+    def squares_on():
+        for i in range(1, NT):
+            sq_copy(i).wait_recv()
+        r.sq_row[x] = sum(r.sq_part[i] for i in range(NT))
+        for k in range(1, NX):
+            sx_copy(k).start()
+
+    def squares_end():
+        for k in range(1, NX):
+            sx_copy(k).wait_recv()
+        for b in range(NX):
+            r.row_scale[b] = column(lax.rsqrt(r.sq_row[b, :1] / dim + EPSILON))
+
 
     def mid_piece(axis, at_x, at_y, own_core, first):
         def ref(k, half):
             of_x = lax.rem(x + at_x + (k if axis == 0 else 0), NX)
             of_y = lax.rem(y + at_y + (k if axis == 1 else 0), NY)
-            where = pl.ds(pl.multiple_of((of_y * NC + own_core) * cols, cols), cols)
+            where = channels(of_y * NC + own_core)
             quarter = rows // 4
             at = pl.ds(first * 2 * quarter, 2 * quarter)
             if half is not None:
@@ -491,6 +586,7 @@
         s[0][0]().start()
     for g, s in second_rings[0]:
         g.start()
+    squares_start()
     for way in range(2):
         for i, (g, s) in enumerate(first_rings):
             g.near(way)
@@ -502,6 +598,7 @@
             g.near(way)
             s[1 + way][0]().start()
     hop_on(2, 1)
+    squares_on()
     for i, (g, s) in enumerate(first_rings):
         for half in range(2):
             g.far(half)
@@ -524,26 +621,38 @@
         for g, s in second_rings[3]:
             g.far(half)
             s[3 + half][0]().start()
-    if far == 2:
-        pass
-    else:
-        hop_on(far)
     rings = first_rings + [pair_of for both_of in second_rings for pair_of in both_of]
     for i, (g, s) in enumerate(rings):
         for j, (out, come) in enumerate(s):
             if j > 0 or i < 2:
                 come().wait_recv()
 
+    def ahead(j):
+        return jnp.where(j == 0, 2, jnp.where(j == 1, 1, jnp.where(j == 2, 3, 0)))
+
+    def early(j, carry):
+        b = lax.rem(x + ahead(j), NX)
+
+        r.gu_sum[b] = wide_dot(r.mid[b, :, cols:], r.gubuf[1:].reshape(dim - cols, 2 * UNIT))
+        return carry
+
+    squares_end()
+    lax.fori_loop(0, EARLY, early, 0)
+    hop_on(far)
+
     def mixer(j):
         b = lax.rem(x + ahead(j), NX)
-        squares = jnp.zeros((rows, 128), F32)
-        for i in range(r.mid.shape[2] // 128):
-            v = r.mid[b, :, i * 128 : (i + 1) * 128].astype(F32)
-            squares = squares + v * v
-        mean = jnp.sum(squares, axis=1, keepdims=True) / r.mid.shape[2]
-        row_scale = lax.rsqrt(mean + EPSILON)
-        mid = r.mid[b]
-        gu = wide_dot(mid, r.gubuf[...].reshape(mid.shape[1], 2 * UNIT)) * row_scale
+
+        @pl.when(j < EARLY)
+        def _():
+            r.gu_sum[b] += wide_dot(r.mid[b, :, :cols], r.gubuf[0].reshape(cols, 2 * UNIT))
+
+        @pl.when(j >= EARLY)
+        def _():
+            r.gu_sum[b] = wide_dot(r.mid[b], r.gubuf[...].reshape(dim, 2 * UNIT))
+
+        gu = r.gu_sum[b]
+        gu = gu * r.row_scale[b]
         gate, mixed_tile, upward = gu[:, :128], gu[:, 128:256], gu[:, 256:]
         first = gate / (1.0 + jnp.exp(-gate)) * upward
         second = (mixed_tile / (1.0 + jnp.exp(-mixed_tile)))[:, :64] * mixed_tile[:, 64:]
@@ -555,9 +664,6 @@
             for c in range(NC):
                 r.part[c, b, :, :, zz * NX * n : (zz + 1) * NX * n] = terms[:, c]
         core_copy(j).start()
-
-    def ahead(j):
-        return jnp.where(j == 0, 2, jnp.where(j == 1, 1, jnp.where(j == 2, 3, 0)))
 
     def core_copy(j):
         b = lax.rem(x + ahead(j), NX)
@@ -603,9 +709,7 @@
         return scatter(4 + j, 0, x, y + ahead(j), 1)
 
     def stage(j, carry):
-        @pl.when(j < NX)
-        def _():
-            mixer(j)
+        mixer(j)
 
         @pl.when(j >= 1)
         def _():
@@ -617,40 +721,41 @@
             for i in range(NY):
                 first_along_x(i).start()
 
-        @pl.when(j >= 2)
-        def _():
-            first_along_y(j - 2).near(0)
-            first_along_y(j - 2).near(1)
-
-        @pl.when(j == NX - 1)
-        def _():
-            for i in range(NY):
-                first_along_x(i).near(0)
-                first_along_x(i).near(1)
-
         return carry
 
-    lax.fori_loop(0, NX + 1, stage, 0)
+    lax.fori_loop(0, NX, stage, 0)
     steps = [[first_along_y(j), first_along_x(j)] for j in range(NX)]
     ends = [scatter(8, 0, x, y, 0), scatter(9, 1, x, y, 1)]
-    first_along_y(NX - 1).near(0)
-    first_along_y(NX - 1).near(1)
+    for h in range(2):
+        first_along_x(0).near(h)
+        first_along_y(0).near(h)
+    core_sum(NX - 1)
+    first_along_y(NX - 1).start()
+    for j in range(1, NX):
+        for h in range(2):
+            first_along_x(j).near(h)
+            first_along_y(j).near(h)
     for j, both_of in enumerate(steps):
         for s in both_of:
             s.finish()
-        if j == 0:
-            for s in ends:
+        for s in ends:
+            if j == 0:
                 s.start()
-    for s in ends:
-        s.near(0)
-        s.near(1)
+            if j == 1:
+                s.near(1)
+            if j == 2:
+                s.near(0)
     own_rows = pl.ds(pl.multiple_of(tp * share, share), share)
     for first, s in enumerate(ends):
         at = slice(first * depth, (first + 1) * depth)
-        r.out[:, at] = (s.total() + r.mid[x, own_rows, at].astype(F32)).astype(BF16)
+        r.out[:, at] = s.total()
+
+    for t in range(NT):
+        r.middle[:, t * cols : (t + 1) * cols] = r.mid[x, own_rows, channels(t)]
 
     for k in range(1, NX):
-        o_copy(k).wait_send()
+        for h in range(2):
+            o_copy(k, h).wait_send()
         s_copy(k).wait_send()
         for copy in weight_copies(k):
             copy.wait_send()
@@ -660,18 +765,26 @@
         for chunk in range(CHUNKS):
             ring(0, slot, chunk, up).wait_send()
             pair(slot, chunk, core).wait_send()
-    for d in range(1, far + 1):
+    for way, part in in_hop(1):
+        for k in range(NX):
+            first_hop(k, way, part).wait_send()
+    for d in range(2, far + 1):
         for way, part in in_hop(d):
             hop(d, way, part).wait_send()
     gq.done()
-    ga.done()
-    for out, come in swaps:
-        out().wait_send()
+    for g, swaps in heads:
+        g.done()
+        for out, come in swaps:
+            out().wait_send()
     for i, (g, s) in enumerate(rings):
         g.done()
         for j, (out, come) in enumerate(s):
             if j > 0 or i < 2:
                 out().wait_send()
+    for i in range(1, NT):
+        sq_copy(i).wait_send()
+    for k in range(1, NX):
+        sx_copy(k).wait_send()
     for j in range(NX):
         core_copy(j).wait_send()
     for both_of in [*steps, ends]:
@@ -716,6 +829,10 @@
         "att": ((rows, NT * 2 * VDIM), BF16),
         "mid": ((NX, rows, dim), BF16),
         "part": ((NC, NX, NY, share, dim), BF16),
+        "row_scale": ((NX, rows, 1), F32),
+        "gu_sum": ((NX, rows, 2 * UNIT), F32),
+        "sq_part": ((NT, 8, rows), F32),
+        "sq_row": ((NX, 8, rows), F32),
         "pairbuf": ((NX, NY, share, dim), BF16),
         "half_in": ((10, 2, share, dim // 4), BF16),
         "whole_in": ((10, 2, share, dim // 2), BF16),
@@ -732,31 +849,40 @@
         "wx_recv": (NX, 2),
         "ow_send": (NT,),
         "ow_recv": (NT,),
+        "first_send": (NX, 2, 2),
+        "first_recv": (NX, 2, 2),
         "hop_send": (nz, 2, 2),
         "hop_recv": (nz, 2, 2),
-        "o_send": (NX,),
-        "o_recv": (NX,),
+        "o_send": (NX, 2),
+        "o_recv": (NX, 2),
         "s_send": (NX,),
         "s_recv": (NX,),
-        "ga_send": (1, 4),
-        "ga_recv": (1, 4),
-        "sa_send": (1, 5),
-        "sa_recv": (1, 5),
+        "ga_send": (2, 4),
+        "ga_recv": (2, 4),
+        "sa_send": (2, 5),
+        "sa_recv": (2, 5),
         "gm_send": (10, 4),
         "gm_recv": (10, 4),
         "sm_send": (10, 5),
         "sm_recv": (10, 5),
+        "sq_send": (NT,),
+        "sq_recv": (NT,),
+        "sx_send": (NX,),
+        "sx_recv": (NX,),
         "pc_send": (NX,),
         "pc_recv": (NX,),
         "rs_send": (10, 4),
         "rs_recv": (10, 4),
     }
-    names = [*inputs, "out", *buffers, *semaphores]
+    names = [*inputs, "out", "middle", *buffers, *semaphores]
     return pl.pallas_call(
         functools.partial(layer_kernel, nz, names),
-        out_shape=jax.ShapeDtypeStruct((share, dim), BF16),
+        out_shape=(
+            jax.ShapeDtypeStruct((share, dim), F32),
+            jax.ShapeDtypeStruct((share, dim), BF16),
+        ),
         in_specs=[anywhere if name in whole else vmem for name in inputs],
-        out_specs=vmem,
+        out_specs=(vmem, vmem),
         scratch_shapes=[pltpu.VMEM(*b) for b in buffers.values()]
         + [pltpu.SemaphoreType.DMA(s) for s in semaphores.values()],
         compiler_params=pltpu.CompilerParams(
@@ -789,7 +915,7 @@
 
     inputs = {
         "latent": latent,
-        "rope_key": rope_key,
+        "rope_key": rope_key.T,
         "queries": queries,
         "lat_gain": lat_gain[None, :],
         "kv_weight": kv_weight,
@@ -803,7 +929,8 @@
         "ow": out_weight,
         "resid": resid,
     }
-    return layer(inputs, ("dn", "ow", "resid"))
+    ffn_sum, middle = layer(inputs, ("dn", "ow", "resid"))
+    return (middle.astype(F32) + ffn_sum).astype(BF16)
 
 
 def solution(mesh):

time: 122 us -> 121 us (level)
  local copies, waits for them, and re-layouts: 3.16 us -> 0 us
  other arithmetic: 0 us -> 1.86 us
    unnamed x2 -> x0, local copies, waits for them, and re-layouts: 3.16 us -> none
    convert_element_type x0 -> x1, other arithmetic: none -> 1.86 us  [body(): return (middle.astype(F32) + ffn_sum).astype(BF16)]
where the time goes in v5:
time: 121 us; the launch traced here: 120 us
  Pallas kernels  119 us (98%)
  other arithmetic  1.86 us (2%)
    pallas_call x1, Pallas kernels, layer(): pl.pallas_call(functools.partial(layer_kernel, nz, names), out_shape=(jax...  119 us

profile of v5, /device:TPU:1, one launch (start us, length us, event | category | flops | bytes accessed | tf_op | source)
XLA Modules:
  0.0 120.4 jit_solution(270975741270588268)
XLA Ops:
  0.0 118.6 %shard_map.136 = (f32[32,4096]{1,0:T(8,128)}, bf16[32,4096]{1,0:T(8,128)(2,1)}) custom-call(bf16[256,512]{1,0:T(8,128)(2,1)} %values_0_.1, bf16[64,256]{1,0:T(8,128)(2,1)} %bitcast.6, bf16[256,384]{1,0:T(8,128)(2,1)} %values_2_.1, f32[1,512]{1,0:T(1,128)} %bitcast.8, bf16[512,512]{1,0:T(8,128)(2,1)} %values_4_.1, bf16[128,768]{1,0:T(8,128)(2,1)} %values_5_.1, ...), custom_call_target="tpu_custom_call" | custom-call | tf_op jit(solution)/shard_map/pallas_call | solution.py:878
  118.6 1.9 %add_convert_fusion = bf16[32,4096]{1,0:T(8,128)(2,1)} fusion(f32[32,4096]{1,0:T(8,128)} %get-tuple-element.8, bf16[32,4096]{1,0:T(8,128)(2,1)} %get-tuple-element.7), kind=kLoop, calls=%fused_computation | loop fusion | flops 393216 | bytes 1048576 | tf_op jit(solution)/shard_map/convert_element_type | solution.py:933

commit v6 on v5

--- a/solution.py
+++ b/solution.py
@@ -428,15 +428,15 @@
         lax.fori_loop(0, 2, both(1), 0)
         hop_latent(3)
     start_first(0)
+    for d in range(2, far - 1):
+        lax.fori_loop(0, 2, both(d), 0)
     start_first(1)
     start_first(3)
-    for d in range(2, far - 1):
-        lax.fori_loop(0, 2, both(d), 0)
-    start_first(2)
     if far > 3:
         hop_latent(4)
     lax.fori_loop(0, 2, both(far - 1), 0)
     use(far, z - far >= 0)
+    start_first(2)
 
     for b in range(NX):
         at = pl.ds(b * rows, rows)
@@ -731,20 +731,21 @@
         first_along_y(0).near(h)
     core_sum(NX - 1)
     first_along_y(NX - 1).start()
-    for j in range(1, NX):
+    for j in range(1, NX - 1):
         for h in range(2):
             first_along_x(j).near(h)
             first_along_y(j).near(h)
-    for j, both_of in enumerate(steps):
-        for s in both_of:
-            s.finish()
-        for s in ends:
-            if j == 0:
-                s.start()
-            if j == 1:
-                s.near(1)
-            if j == 2:
-                s.near(0)
+    for both_of, s in zip(steps[0], ends, strict=True):
+        both_of.finish()
+        s.start()
+    for h in range(2):
+        first_along_x(NX - 1).near(h)
+        first_along_y(NX - 1).near(h)
+    for j in range(1, NX):
+        for both_of, s in zip(steps[j], ends, strict=True):
+            both_of.finish()
+            if j < NX - 1:
+                s.near(1 if j == 1 else 0)
     own_rows = pl.ds(pl.multiple_of(tp * share, share), share)
     for first, s in enumerate(ends):
         at = slice(first * depth, (first + 1) * depth)

time: 121 us -> 119 us (0.983)
  Pallas kernels: 119 us -> 117 us
    pallas_call x1, Pallas kernels: 119 us -> 117 us  [layer(): pl.pallas_call(functools.partial(layer_kernel, nz, names), out_shape=(jax...]
where the time goes in v6:
time: 119 us
  Pallas kernels  117 us (98%)
  other arithmetic  1.86 us (2%)
    pallas_call x1, Pallas kernels, layer(): pl.pallas_call(functools.partial(layer_kernel, nz, names), out_shape=(jax...  117 us

profile of v6, /device:TPU:1, one launch (start us, length us, event | category | flops | bytes accessed | tf_op | source)
XLA Modules:
  0.0 118.9 jit_solution(5078654497725775063)
XLA Ops:
  0.0 117.1 %shard_map.136 = (f32[32,4096]{1,0:T(8,128)}, bf16[32,4096]{1,0:T(8,128)(2,1)}) custom-call(bf16[256,512]{1,0:T(8,128)(2,1)} %values_0_.1, bf16[64,256]{1,0:T(8,128)(2,1)} %bitcast.6, bf16[256,384]{1,0:T(8,128)(2,1)} %values_2_.1, f32[1,512]{1,0:T(1,128)} %bitcast.8, bf16[512,512]{1,0:T(8,128)(2,1)} %values_4_.1, bf16[128,768]{1,0:T(8,128)(2,1)} %values_5_.1, ...), custom_call_target="tpu_custom_call" | custom-call | tf_op jit(solution)/shard_map/pallas_call | solution.py:879
  117.1 1.9 %add_convert_fusion = bf16[32,4096]{1,0:T(8,128)(2,1)} fusion(f32[32,4096]{1,0:T(8,128)} %get-tuple-element.8, bf16[32,4096]{1,0:T(8,128)(2,1)} %get-tuple-element.7), kind=kLoop, calls=%fused_computation | loop fusion | flops 393216 | bytes 1048576 | tf_op jit(solution)/shard_map/convert_element_type | solution.py:934

commit v7 on v6

--- a/solution.py
+++ b/solution.py
@@ -183,8 +183,11 @@
         pltpu.make_async_copy(r.resid.at[:, own_cols], r.residbuf, r.local_sem.at[2]),
         pltpu.make_async_copy(r.gustage.at[x], r.gubuf.at[far, x], r.local_sem.at[3]),
         pltpu.make_async_copy(r.owstage.at[:, own_cols], r.owbuf.at[tp], r.local_sem.at[4]),
+        pltpu.make_async_copy(r.gate, r.gate_here, r.local_sem.at[5]),
+        pltpu.make_async_copy(r.upward, r.up_here, r.local_sem.at[6]),
+        pltpu.make_async_copy(r.kv_weight, r.kv_here, r.local_sem.at[7]),
     ]
-    for copy in local[:3]:
+    for copy in local[5:] + local[:3]:
         copy.start()
 
     half = ROPE // 2
@@ -239,7 +242,9 @@
     gq.start()
 
     gain = column(r.ffn_gain[pl.ds(sp, 1), :])
-    gate, upward = r.gate[...].astype(F32) * gain, r.upward[...].astype(F32) * gain
+    for copy in local[5:]:
+        copy.wait()
+    gate, upward = r.gate_here[...].astype(F32) * gain, r.up_here[...].astype(F32) * gain
     for i in range(NX):
         lo, mid_lo, hi = i * UNIT, i * UNIT + 128, (i + 1) * UNIT
         tiles = [gate[:, lo:mid_lo], gate[:, mid_lo:hi], upward[:, mid_lo:hi], upward[:, lo:mid_lo]]
@@ -250,8 +255,8 @@
             copy.start()
     for h in range(2):
         at = 2 * h * NOPE
-        r.wk[:, h * NOPE : (h + 1) * NOPE] = r.kv_weight[:, at : at + NOPE]
-        value_weight = r.kv_weight[:, at + NOPE : at + NOPE + VDIM].astype(F32)
+        r.wk[:, h * NOPE : (h + 1) * NOPE] = r.kv_here[:, at : at + NOPE]
+        value_weight = r.kv_here[:, at + NOPE : at + NOPE + VDIM].astype(F32)
         r.wv[h * VDIM : (h + 1) * VDIM, :] = jnp.transpose(value_weight).astype(BF16)
     local[0].wait()
     gain = column(r.out_gain[...])
@@ -814,6 +819,9 @@
         "stat_a": ((2, 1, NX * rows), F32),
         "wk": ((wide, 2 * NOPE), BF16),
         "wv": ((heads, wide), BF16),
+        "gate_here": (inputs["gate"].shape, BF16),
+        "up_here": (inputs["upward"].shape, BF16),
+        "kv_here": (inputs["kv_weight"].shape, BF16),
         "gustage": (gu, BF16),
         "owstage": ((heads, dim), BF16),
         "acc": ((2, VDIM, NX * rows), F32),
@@ -839,7 +847,7 @@
         "whole_in": ((10, 2, share, dim // 2), BF16),
     }
     semaphores = {
-        "local_sem": (5,),
+        "local_sem": (8,),
         "ring_send": (nz, CHUNKS),
         "ring_recv": (nz, CHUNKS),
         "pair_send": (nz, CHUNKS),
@@ -930,7 +938,7 @@
         "ow": out_weight,
         "resid": resid,
     }
-    ffn_sum, middle = layer(inputs, ("dn", "ow", "resid"))
+    ffn_sum, middle = layer(inputs, ("dn", "ow", "resid", "gate", "upward", "kv_weight"))
     return (middle.astype(F32) + ffn_sum).astype(BF16)
 
 

time: 119 us -> 119 us (level)
  no operation moved by 1% of the time
where the time goes in v7:
time: 119 us
  Pallas kernels  117 us (98%)
  other arithmetic  1.86 us (2%)
    pallas_call x1, Pallas kernels, layer(): pl.pallas_call(functools.partial(layer_kernel, nz, names), out_shape=(jax...  117 us

profile of v7, /device:TPU:1, one launch (start us, length us, event | category | flops | bytes accessed | tf_op | source)
XLA Modules:
  0.0 118.7 jit_solution(2822112489161713392)
XLA Ops:
  0.0 116.8 %shard_map.136 = (f32[32,4096]{1,0:T(8,128)}, bf16[32,4096]{1,0:T(8,128)(2,1)}) custom-call(bf16[256,512]{1,0:T(8,128)(2,1)} %values_0_.1, bf16[64,256]{1,0:T(8,128)(2,1)} %bitcast.6, bf16[256,384]{1,0:T(8,128)(2,1)} %values_2_.1, f32[1,512]{1,0:T(1,128)} %bitcast.8, bf16[512,512]{1,0:T(8,128)(2,1)} %values_4_.1, bf16[128,768]{1,0:T(8,128)(2,1)} %values_5_.1, ...), custom_call_target="tpu_custom_call" | custom-call | tf_op jit(solution)/shard_map/pallas_call | solution.py:887
  116.8 1.9 %add_convert_fusion = bf16[32,4096]{1,0:T(8,128)(2,1)} fusion(f32[32,4096]{1,0:T(8,128)} %get-tuple-element.8, bf16[32,4096]{1,0:T(8,128)(2,1)} %get-tuple-element.7), kind=kLoop, calls=%fused_computation | loop fusion | flops 393216 | bytes 1048576 | tf_op jit(solution)/shard_map/convert_element_type | solution.py:942
